TPU v7x, 32 devices: a whole 2x2x4 slice. The times are simulated.
32 devices in a mesh: sp: 16 (over z, y, x), tp: 2 (over core).
Axes of the slice: x: 2, y: 2, z: 4, core: 2. Of those that a mesh axis runs over, the one named last changes fastest.
Arguments:
- value_in: bfloat16 [5760, 2048], P('sp', 'tp'), may hold values from -240 to 240
- gate_in: bfloat16 [5760, 2048], P('sp', 'tp'), may hold values from -8 to 8
- taps: float32 [31, 2048], P(None, 'tp'), may hold values from -1 to 1
- norm_gain: float32 [2048], P('tp'), may hold values from 0.1 to 1.9
- norm_bias: float32 [2048], P('tp'), may hold values from -3 to 3
- proj_weight: bfloat16 [2048, 4096], P('tp', 'sp'), may hold values from -0.125 to 0.125
- out_grad: bfloat16 [5760, 4096], P('sp'), may hold values from -6 to 6
Outputs:
- value_grad: bfloat16 [5760, 2048], P('sp', 'tp')
- gate_grad: bfloat16 [5760, 2048], P('sp', 'tp')
- tap_grad: float32 [31, 2048], P(None, 'tp')
- gain_grad: float32 [2048], P('tp')
- bias_grad: float32 [2048], P('tp')
- weight_grad: float32 [2048, 4096], P('tp', 'sp')
All inputs are finite; a program needn't handle non-finite values.
Results may differ from a plain program's by a relative error of at most 0.0051.
Values may be sent and summed in bfloat16 or wider, within the bound.
A program may use at most 64 MiB of HBM per device.

v0:
```python
import functools
import jax
import jax.numpy as jnp
from jax import lax
from jax.experimental import pallas as pl
from jax.experimental.pallas import tpu as pltpu
from jax.sharding import PartitionSpec as P


def padded_rows(cells, width):
    count = lax.axis_size("sp")
    ends = count - 1
    rows = cells.shape[0]
    before = lax.ppermute(cells[rows - width :], "sp", [(i, i + 1) for i in range(ends)])
    after = lax.ppermute(cells[:width], "sp", [(i + 1, i) for i in range(ends)])
    return jnp.concatenate([before, cells, after], axis=0)


def on_device(*arrays):
    return compute(*arrays)


def compute(value_in, gate_in, taps, norm_gain, norm_bias, proj_weight, out_grad):
    f32, bf16 = jnp.float32, jnp.bfloat16
    rows, local_width = value_in.shape
    span = taps.shape[0]
    half = span // 2
    tp = lax.axis_size("tp")
    count = lax.axis_size("sp")
    inner = 1 << ((count.bit_length() - 1) // 2)
    outer = count // inner
    width_all = local_width * tp
    block = proj_weight.shape[1]
    me = lax.axis_index("sp")
    plane, place = me // inner, me % inner
    core = lax.axis_index("tp")

    def swap(array, d):
        return lax.ppermute(
            array, "sp", [(i, i - i % inner + ((i % inner) ^ d)) for i in range(count)]
        )

    def shift(array, e):
        return lax.ppermute(array, "sp", [(i, (i + e * inner) % count) for i in range(count)])

    def across(array, t):
        return lax.ppermute(array, "tp", [(c, c ^ t) for c in range(tp)])

    def tp_sum(array):
        return array + sum(across(array, t) for t in range(1, tp))

    gate_sig = jax.nn.sigmoid(gate_in.astype(f32))
    value_f = value_in.astype(f32)
    mixed = (value_f * gate_sig).astype(bf16)
    padded = padded_rows(mixed, half).astype(f32)

    def columns_of(where, first, blocks):
        return jnp.concatenate(
            [
                lax.dynamic_slice_in_dim(
                    out_grad,
                    (((plane + first + e) % outer) * inner + where) * block,
                    block,
                    axis=1,
                )
                for e in range(blocks)
            ],
            axis=1,
        )

    share = outer // tp
    own_columns = columns_of(place, 0, outer)
    arrived = [swap(columns_of(place ^ d, core * share, share), d) for d in range(1, inner)]
    weights = [proj_weight] + [shift(proj_weight, -e) for e in range(1, outer)]
    weight_cols = jnp.concatenate(weights, axis=1)
    cotangents = [own_columns]
    for got in arrived:
        parts = jnp.stack([got] + [across(got, t) for t in range(1, tp)])
        cotangents.append(
            jnp.concatenate(
                [
                    lax.dynamic_index_in_dim(parts, core ^ j, axis=0, keepdims=False)
                    for j in range(tp)
                ],
                axis=1,
            )
        )

    conv = jnp.zeros((rows, local_width), f32)
    for k in range(span):
        conv = conv + taps[k] * padded[k : k + rows]
    mean = tp_sum(jnp.sum(conv, axis=1)) / width_all
    centred = conv - mean[:, None]
    spread = tp_sum(jnp.sum(centred * centred, axis=1)) / width_all
    inv = lax.rsqrt(spread + 1e-06)
    normed = centred * inv[:, None]
    pre = normed * norm_gain + norm_bias
    sig_pre = jax.nn.sigmoid(pre)
    act = (pre * sig_pre).astype(bf16)
    acts = [act] + [swap(act, d) for d in range(1, inner)]

    partial = [
        lax.dot_general(c, weight_cols, (((1,), (1,)), ((), ())), preferred_element_type=f32)
        for c in cotangents
    ]
    act_grad = partial[0]
    sending = lax.optimization_barrier(([p.astype(bf16) for p in partial[1:]], acts))[0]
    for d in range(1, inner):
        got = swap(sending[d - 1], d)
        act_grad = act_grad + got.astype(f32)

    pre_grad = act_grad * sig_pre * (1.0 + pre * (1.0 - sig_pre))
    normed_grad = pre_grad * norm_gain
    sums = tp_sum(
        jnp.stack([jnp.sum(normed_grad, axis=1), jnp.sum(normed_grad * normed, axis=1)])
    )
    first, second = sums[0], sums[1]
    conv_grad = inv[:, None] * (
        normed_grad - first[:, None] / width_all - normed * second[:, None] / width_all
    )
    extended = lax.optimization_barrier(padded_rows(conv_grad, half))
    tap_local = jnp.stack([jnp.sum(conv_grad * padded[k : k + rows], axis=0) for k in range(span)])
    gain_local = jnp.sum(pre_grad * normed, axis=0)
    bias_local = jnp.sum(pre_grad, axis=0)
    small = jnp.concatenate([tap_local, gain_local[None], bias_local[None]], axis=0)
    small = small + sum(swap(small, d) for d in range(1, inner))
    small = small + sum(shift(small, e) for e in range(1, outer))
    tap_grad, gain_grad, bias_grad = small[:span], small[span], small[span + 1]

    mixed_grad = jnp.zeros((rows, local_width), f32)
    for k in range(span):
        mixed_grad = mixed_grad + taps[k] * extended[2 * half - k : 2 * half - k + rows]
    value_grad = (mixed_grad * gate_sig).astype(bf16)
    gate_grad = (mixed_grad * value_f * gate_sig * (1.0 - gate_sig)).astype(bf16)

    weight_part = lax.dot_general(
        jnp.concatenate(acts, axis=0),
        jnp.concatenate(cotangents, axis=0),
        (((0,), (0,)), ((), ())),
        preferred_element_type=f32,
    )
    weight_grad = weight_part[:, :block]
    for e in range(1, outer):
        sent = weight_part[:, e * block : (e + 1) * block].astype(bf16)
        got = shift(sent, e)
        weight_grad = weight_grad + got.astype(f32)
    return (value_grad, gate_grad, tap_grad, gain_grad, bias_grad, weight_grad)


LANES = 128
EDGE = 16
MESH = pl.DeviceIdType.MESH


def slot_table(planes, blocks):
    parts = blocks // 2
    sizes = {
        "halo": 2,
        "cols_x": parts,
        "cols_x_core": parts,
        "cols_d": parts,
        "cols_d_core": parts,
        "cols_y": parts,
        "cols_y_core": parts,
        "w_y": 1,
        "w_up": 2 * (planes - 1),
        "w_down": 2 * (planes - 1),
        "stats": 1,
        "act_x": 1,
        "act_y": 1,
        "act_d": 1,
        "part_x": 2,
        "part_y": 1,
        "up": blocks,
        "down": blocks,
        "w_back": 1,
        "norm": 1,
        "grad_halo": 2,
        "plane_in": 3,
        "across": planes,
        "plane_out": 3,
    }
    first, total = {}, 0
    for name, size in sizes.items():
        first[name] = total
        total += size
    return first, total


def kernel(
    shape,
    first,
    value,
    gate,
    taps,
    gain,
    bias,
    weight,
    cotangent,
    value_grad,
    gate_grad,
    tap_grad,
    gain_grad,
    bias_grad,
    weight_grad,
    value_v,
    gate_v,
    cols,
    wh,
    tap_t,
    mixed,
    edge_out,
    edge_in,
    conv,
    dact,
    stat_out,
    stat_in,
    rows_of,
    acts,
    factor_v,
    factor_g,
    part,
    part_out,
    part_in,
    half_out,
    half_in,
    wg,
    up_out,
    down_out,
    up_in,
    down_in,
    back_out,
    back_in,
    grads,
    gedge_out,
    gedge_in,
    small,
    plane_in,
    across,
    owned,
    small_all,
    tile,
    send_sem,
    recv_sem,
    local_sem,
):
    rows, width, span, planes, block, step = shape
    f32, bf16 = jnp.float32, jnp.bfloat16
    blocks = 2 * planes
    parts = blocks // 2
    side = width // 2
    tiles = width // LANES
    tiles_side = tiles // 2
    quarter = tiles // 4
    count = 4 * planes
    half = span // 2
    lead = EDGE - half

    me, core = lax.axis_index("sp"), lax.axis_index("tp")
    z, y, x = lax.div(me, 4), lax.rem(lax.div(me, 2), 2), lax.rem(me, 2)
    yn, xn = 1 - y, 1 - x

    def at(zz, yy, xx):
        return (zz * 4 + yy * 2 + xx, core)

    to_x, to_y, to_d = at(z, y, xn), at(z, yn, x), at(z, yn, xn)
    to_core = (me, 1 - core)
    to_up, to_down = (me + 4, core), (me - 4, core)
    to_next, to_prev = (me + 1, core), (me - 1, core)
    has_up, has_down = z < planes - 1, z > 0
    has_next, has_prev = me < count - 1, me > 0

    pending = []

    def copy(src, dst, name, index, device):
        at_slot = first[name] + index
        return pltpu.make_async_remote_copy(
            src_ref=src,
            dst_ref=dst,
            send_sem=send_sem.at[at_slot],
            recv_sem=recv_sem.at[at_slot],
            device_id=device,
            device_id_type=MESH,
        )

    def send(made, when=None):
        pending.append((made, when))
        if when is None:
            made.start()
        else:
            pl.when(when)(made.start)

    def arrive(made, when=None):
        if when is None:
            made.wait_recv()
        else:
            pl.when(when)(made.wait_recv)

    def lanes(j):
        return pl.ds(pl.multiple_of(j * LANES, LANES), LANES)

    def over(n, body):
        def step_of(j, carry):
            body(j)
            return carry

        lax.fori_loop(0, n, step_of, 0)

    my_rows = pl.ds(pl.multiple_of(y * side, side), side)
    their_rows = pl.ds(pl.multiple_of(yn * side, side), side)

    def column(b):
        return pl.ds(pl.multiple_of(b * block, block), block)

    def index_of(c, q):
        return c * (blocks - 1) + q * (1 - 2 * c)

    mine = [index_of(core, q) for q in range(parts)]
    other = [index_of(1 - core, q) for q in range(parts)]

    load_v = pltpu.make_async_copy(value, value_v, local_sem.at[0])
    load_g = pltpu.make_async_copy(gate, gate_v, local_sem.at[1])
    load_w = pltpu.make_async_copy(weight.at[my_rows], wh.at[z * 2 + y], local_sem.at[2])
    load_c = [
        pltpu.make_async_copy(
            cotangent.at[:, column(2 * i + x)], cols.at[0, i], local_sem.at[3 + i]
        )
        for i in range(blocks)
    ]
    load_v.start()
    load_g.start()

    barrier = pltpu.get_barrier_semaphore()
    peers = [to_x, to_y, to_d, to_core]
    peers += [at(lax.rem(z + d, planes), y, x) for d in range(1, planes)]
    peers += [(lax.rem(me + 1, count), core), (lax.rem(me + count - 1, count), core)]
    for peer in peers:
        pl.semaphore_signal(barrier, inc=1, device_id=peer, device_id_type=MESH)
    pl.semaphore_wait(barrier, len(peers))

    def w_copies(d, p):
        yb = y if p == 0 else yn
        index = 2 * (d - 1) + p
        below = wh.at[lax.rem(z - d + planes, planes) * 2 + yb]
        above = wh.at[lax.rem(z + d, planes) * 2 + yb]
        return (
            copy(below, below, "w_up", index, to_up),
            copy(above, above, "w_down", index, to_down),
        )

    def w_first(p, src, yb):
        dst = wh.at[z * 2 + yb]
        send(copy(src, dst, "w_up", p, to_up), has_up)
        send(copy(src, dst, "w_down", p, to_down), has_down)

    def w_forward(d, p):
        up, down = w_copies(d, p)
        yb = y if p == 0 else yn
        below = wh.at[lax.rem(z - d + planes, planes) * 2 + yb]
        above = wh.at[lax.rem(z + d, planes) * 2 + yb]
        arrive(up, z >= d)
        if d < planes - 1:
            send(copy(below, below, "w_up", 2 * d + p, to_up), jnp.logical_and(z >= d, has_up))
        arrive(down, z + d < planes)
        if d < planes - 1:
            send(
                copy(above, above, "w_down", 2 * d + p, to_down),
                jnp.logical_and(z + d < planes, has_down),
            )

    w_first(0, weight.at[my_rows], y)
    w_y = copy(weight.at[their_rows], wh.at[z * 2 + y], "w_y", 0, to_y)
    send(w_y)

    def cols_x(q):
        return copy(
            cotangent.at[:, column(2 * mine[q] + xn)], cols.at[1, mine[q]], "cols_x", q, to_x
        )

    def cols_d(q):
        return copy(cols.at[1, mine[q]], cols.at[3, mine[q]], "cols_d", q, to_y)

    def cols_y(q):
        return copy(
            cotangent.at[:, column(2 * mine[q] + x)], cols.at[2, mine[q]], "cols_y", q, to_y
        )

    def cols_core(slab, name, q):
        ref = cols.at[slab, mine[q]]
        return copy(ref, ref, name, q, to_core)

    def pass_x(q):
        arrive(cols_x(q))
        send(cols_d(q))
        send(cols_core(1, "cols_x_core", q))

    def pass_d(q):
        arrive(cols_d(q))
        send(cols_core(3, "cols_d_core", q))

    def pass_y(q):
        arrive(cols_y(q))
        send(cols_core(2, "cols_y_core", q))

    send(cols_x(0))

    def lay_taps(j):
        tap_t[j, 0:span, :] = taps[:, lanes(j)]
        small[j] = jnp.zeros(small.shape[1:], f32)

    over(tiles, lay_taps)
    load_v.wait()
    load_g.wait()

    def gate_tile(j):
        sig = jax.nn.sigmoid(gate_v[:, lanes(j)].astype(f32))
        got = (value_v[:, lanes(j)].astype(f32) * sig).astype(bf16).astype(f32)
        mixed[j, EDGE : EDGE + rows, :] = got
        edge_out[0, j] = mixed[j, rows : rows + EDGE, :].astype(bf16)
        edge_out[1, j] = mixed[j, EDGE : 2 * EDGE, :].astype(bf16)

    over(tiles, gate_tile)
    halo_prev = copy(edge_out.at[0], edge_in.at[0], "halo", 0, to_next)
    halo_next = copy(edge_out.at[1], edge_in.at[1], "halo", 1, to_prev)
    send(halo_prev, has_next)
    send(halo_next, has_prev)
    for q in range(1, parts):
        send(cols_x(q))
    load_w.start()
    for made in load_c:
        made.start()

    def fill(made, when, src, dst, at_row):
        @pl.when(when)
        def _():
            made.wait_recv()
            for j in range(tiles):
                dst[j, at_row : at_row + EDGE, :] = src[j].astype(f32)

        @pl.when(jnp.logical_not(when))
        def _():
            for j in range(tiles):
                dst[j, at_row : at_row + EDGE, :] = jnp.zeros((EDGE, LANES), f32)

    fill(halo_prev, has_prev, edge_in.at[0], mixed, 0)
    fill(halo_next, has_next, edge_in.at[1], mixed, EDGE + rows)

    def conv_tile(j):
        for r in range(0, rows, step):
            acc = tap_t[j, 0:1, :] * mixed[j, r + lead : r + lead + step, :]
            for k in range(1, span):
                at_row = r + k + lead
                acc = acc + tap_t[j, k : k + 1, :] * mixed[j, at_row : at_row + step, :]
            conv[j, r : r + step, :] = acc

    over(tiles, conv_tile)
    pass_x(0)
    arrive(w_y)
    w_first(1, wh.at[z * 2 + yn], yn)
    w_forward(1, 0)

    for r in range(0, rows, step):
        at_rows = slice(r, r + step)
        total = conv[0, at_rows, :]
        for j in range(1, tiles):
            total = total + conv[j, at_rows, :]
        middle = jnp.sum(total, axis=1, keepdims=True) / width
        off = conv[0, at_rows, :] - middle
        square = off * off
        for j in range(1, tiles):
            off = conv[j, at_rows, :] - middle
            square = square + off * off
        stat_out[0, at_rows, :] = total
        stat_out[1, at_rows, :] = square
    stats = copy(stat_out.at[0:2], stat_in.at[0:2], "stats", 0, to_core)
    send(stats)
    pass_x(1) if parts > 1 else None
    arrive(stats)
    for r in range(0, rows, step):
        at_rows = slice(r, r + step)
        here = jnp.sum(stat_out[0, at_rows, :], axis=1, keepdims=True)
        there = jnp.sum(stat_in[0, at_rows, :], axis=1, keepdims=True)
        both = stat_out[1, at_rows, :] + stat_in[1, at_rows, :]
        apart = (here - there) / width
        spread = jnp.sum(both, axis=1, keepdims=True) / (2 * width) + apart * apart / 4
        inv = lax.rsqrt(spread + 1e-06)
        rows_of[0, at_rows, :] = jnp.broadcast_to((here + there) / (2 * width), (step, LANES))
        rows_of[1, at_rows, :] = jnp.broadcast_to(inv, (step, LANES))

    def act_side(h):
        def act_tile(jj):
            j = h * tiles_side + jj
            normed = (conv[j] - rows_of[0]) * rows_of[1]
            pre = normed * gain[0:1, lanes(j)] + bias[0:1, lanes(j)]
            sig = jax.nn.sigmoid(pre)
            acts[h, :, lanes(jj)] = (pre * sig).astype(bf16)
            conv[j] = normed
            dact[j] = sig * (1.0 + pre * (1.0 - sig))

        over(tiles_side, act_tile)

    act_y = copy(acts.at[yn], acts.at[3], "act_y", 0, to_y)
    act_x = copy(acts.at[y], acts.at[2], "act_x", 0, to_x)
    act_d = copy(acts.at[3], acts.at[4], "act_d", 0, to_x)
    act_side(yn)
    send(act_y)
    act_side(y)
    send(act_x)
    w_forward(1, 1)
    for q in range(2, parts):
        pass_x(q)
    for q in range(parts):
        send(cols_y(q))
    if planes > 2:
        w_forward(2, 0)

    def factor_tile(j):
        sig = jax.nn.sigmoid(gate_v[:, lanes(j)].astype(f32))
        factor_v[j] = sig
        factor_g[j] = value_v[:, lanes(j)].astype(f32) * sig * (1.0 - sig)

    over(tiles, factor_tile)
    if planes > 2:
        w_forward(2, 1)
    arrive(act_y)
    send(act_d)
    for d in range(3, planes):
        w_forward(d, 0)
    for q in range(parts):
        pass_d(q)
    for d in range(3, planes):
        w_forward(d, 1)
    load_w.wait()
    for made in load_c:
        made.wait()

    def product(slab):
        def one(i):
            got = lax.dot_general(
                cols[slab, i], wh[i], (((1,), (1,)), ((), ())), preferred_element_type=f32
            )
            part[slab] = part[slab] + got

        part[slab] = lax.dot_general(
            cols[slab, 0], wh[0], (((1,), (1,)), ((), ())), preferred_element_type=f32
        )
        lax.fori_loop(1, blocks, lambda i, c: (one(i), c)[1], 0)

    part_x = [copy(part_out.at[n], part_in.at[n], "part_x", n, to_x) for n in range(2)]

    def partial(slab, n):
        product(slab)
        part_out[n] = part[slab].astype(bf16)
        send(part_x[n])

    for q in range(parts):
        arrive(cols_core(3, "cols_d_core", q))
    partial(3, 1)
    for q in range(parts):
        arrive(cols_core(1, "cols_x_core", q))
    partial(1, 0)

    arrive(act_x)
    arrive(act_d)

    def weight_of(i):
        acc = None
        for slab, where in enumerate((y, 2, 3, 4)):
            got = lax.dot_general(
                acts[where],
                cols[slab, i],
                (((0,), (0,)), ((), ())),
                preferred_element_type=f32,
            )
            acc = got if acc is None else acc + got
        wg[i] = acc

    for q in range(parts):
        pass_y(q)
        weight_of(mine[q])
        arrive(cols_core(2, "cols_y_core", q))
        weight_of(other[q])

    def up_copy(t, p):
        i = 2 * t + (yn if p == 0 else y)
        return copy(up_out.at[i], up_in.at[i], "up", 2 * t + p, to_up)

    def down_copy(t, p):
        i = 2 * t + (yn if p == 0 else y)
        return copy(down_out.at[i], down_in.at[i], "down", 2 * t + p, to_down)

    def relay(t, p, made, out, got, going, fresh):
        i = 2 * t + (yn if p == 0 else y)

        @pl.when(jnp.logical_and(going, fresh))
        def _():
            out[i] = wg[i].astype(bf16)

        @pl.when(jnp.logical_and(going, jnp.logical_not(fresh)))
        def _():
            made.wait_recv()
            out[i] = (wg[i] + got[i].astype(f32)).astype(bf16)

        send(made, going)

    def serve(m, p):
        t = planes - 1 - m
        relay(t, p, up_copy(t, p), up_out, up_in, z < t, z == 0)
        relay(m, p, down_copy(m, p), down_out, down_in, z > m, z == planes - 1)

    product(2)
    serve(0, 0)
    arrive(part_x[1])
    half_out[...] = (part[2] + part_in[1].astype(f32)).astype(bf16)
    part_y = copy(half_out, half_in, "part_y", 0, to_y)
    send(part_y)
    product(0)
    serve(0, 1)
    arrive(part_x[0])

    stat_out[2] = jnp.zeros((rows, LANES), f32)
    stat_out[3] = jnp.zeros((rows, LANES), f32)

    def back_tile(j, got):
        pre_grad = got * dact[j]
        normed = conv[j]
        scaled = pre_grad * gain[0:1, lanes(j)]
        crossed = pre_grad * normed
        dact[j] = scaled
        stat_out[2] = stat_out[2] + scaled
        stat_out[3] = stat_out[3] + scaled * normed
        small[j, span : span + 1, :] = jnp.sum(crossed, axis=0, keepdims=True)
        small[j, span + 1 : span + 2, :] = jnp.sum(pre_grad, axis=0, keepdims=True)

    def back_mine(jj):
        got = part[0, :, lanes(jj)] + part_in[0, :, lanes(jj)].astype(f32)
        back_tile(y * tiles_side + jj, got)

    def back_theirs(jj):
        back_tile(yn * tiles_side + jj, half_in[:, lanes(jj)].astype(f32))

    over(tiles_side, back_mine)
    arrive(part_y)
    over(tiles_side, back_theirs)
    norm = copy(stat_out.at[2:4], stat_in.at[2:4], "norm", 0, to_core)
    send(norm)
    if planes > 2:
        serve(1, 0)
    arrive(norm)
    for r in range(0, rows, step):
        at_rows = slice(r, r + step)
        for n in range(2):
            both = stat_out[2 + n, at_rows, :] + stat_in[2 + n, at_rows, :]
            got = jnp.sum(both, axis=1, keepdims=True) / (2 * width)
            rows_of[2 + n, at_rows, :] = jnp.broadcast_to(got, (step, LANES))

    def grad_tile(j):
        grads[j, EDGE : EDGE + rows, :] = rows_of[1] * (
            dact[j] - rows_of[2] - conv[j] * rows_of[3]
        )
        gedge_out[0, j] = grads[j, rows : rows + EDGE, :]
        gedge_out[1, j] = grads[j, EDGE : 2 * EDGE, :]

    over(tiles, grad_tile)
    grad_prev = copy(gedge_out.at[0], gedge_in.at[0], "grad_halo", 0, to_next)
    grad_next = copy(gedge_out.at[1], gedge_in.at[1], "grad_halo", 1, to_prev)
    send(grad_prev, has_next)
    send(grad_next, has_prev)

    def tap_tile(j):
        def block_of(r, acc):
            base = pl.multiple_of(r * step, 8)
            own = grads[j, pl.ds(base + EDGE, step), :]
            out = []
            for k in range(span):
                got = own * mixed[j, pl.ds(base + k + lead, step), :]
                out.append(acc[k] + jnp.sum(got.reshape(step // 8, 8, LANES), axis=0))
            return tuple(out)

        start = tuple(jnp.zeros((8, LANES), f32) for _ in range(span))
        acc = lax.fori_loop(0, rows // step, block_of, start)
        for k in range(span):
            small[j, k : k + 1, :] = jnp.sum(acc[k], axis=0, keepdims=True)

    over(tiles, tap_tile)

    place = 2 * y + x
    near = [(to_x, 2 * y + xn), (to_y, 2 * yn + x), (to_d, 2 * yn + xn)]
    own_tiles = pl.ds(place * quarter, quarter)
    gather = [
        copy(small.at[pl.ds(p * quarter, quarter)], plane_in.at[n], "plane_in", n, dev)
        for n, (dev, p) in enumerate(near)
    ]
    for made in gather:
        send(made)
    if planes > 2:
        serve(1, 1)
    fill(grad_prev, has_prev, gedge_in.at[0], grads, 0)
    fill(grad_next, has_next, gedge_in.at[1], grads, EDGE + rows)

    def mixed_tile(j):
        for r in range(0, rows, step):
            at_row = r + EDGE + half
            acc = tap_t[j, 0:1, :] * grads[j, at_row : at_row + step, :]
            for k in range(1, span):
                at_row = r + EDGE + half - k
                acc = acc + tap_t[j, k : k + 1, :] * grads[j, at_row : at_row + step, :]
            tile[r : r + step, :] = acc
        got = tile[...]
        value_grad[:, lanes(j)] = (got * factor_v[j]).astype(bf16)
        gate_grad[:, lanes(j)] = (got * factor_g[j]).astype(bf16)

    def mixed_tiles(lo, hi):
        lax.fori_loop(lo, hi, lambda j, c: (mixed_tile(j), c)[1], 0)

    mixed_tiles(0, tiles_side)
    for made in gather:
        arrive(made)
    across[z] = small[own_tiles] + plane_in[0] + plane_in[1] + plane_in[2]
    for d in range(1, planes):
        made = copy(across.at[z], across.at[z], "across", d, at(lax.rem(z + d, planes), y, x))
        send(made)
    for m in range(2, planes - 1):
        serve(m, 0)
    mixed_tiles(tiles_side, tiles)
    for d in range(1, planes):
        arrive(copy(across.at[z], across.at[z], "across", d, to_core))
    total = across[0]
    for d in range(1, planes):
        total = total + across[d]
    owned[...] = total
    small_all[own_tiles] = total
    spread_out = [
        copy(owned, small_all.at[own_tiles], "plane_out", n, dev) for n, (dev, p) in enumerate(near)
    ]
    for made in spread_out:
        send(made)
    for m in range(2, planes - 1):
        serve(m, 1)

    def finish(p):
        i = 2 * z + (yn if p == 0 else y)
        for t in range(planes):

            @pl.when(z == t)
            def _():
                total = wg[i]
                if t > 0:
                    up_copy(t, p).wait_recv()
                    total = total + up_in[i].astype(f32)
                if t < planes - 1:
                    down_copy(t, p).wait_recv()
                    total = total + down_in[i].astype(f32)
                if p == 0:
                    back_out[...] = total.astype(bf16)
                else:
                    weight_grad[my_rows, :] = total

    finish(0)
    back = copy(back_out, back_in, "w_back", 0, to_y)
    send(back)
    for made in spread_out:
        arrive(made)
    for j in range(tiles):
        tap_grad[:, j * LANES : (j + 1) * LANES] = small_all[j, 0:span, :]
        gain_grad[:, j * LANES : (j + 1) * LANES] = small_all[j, span : span + 1, :]
        bias_grad[:, j * LANES : (j + 1) * LANES] = small_all[j, span + 1 : span + 2, :]
    finish(1)
    arrive(back)
    weight_grad[their_rows, :] = back_in[...].astype(f32)
    for made, when in pending:
        if when is None:
            made.wait_send()
        else:
            pl.when(when)(made.wait_send)


def fused_on_device(value_in, gate_in, taps, norm_gain, norm_bias, proj_weight, out_grad):
    f32, bf16 = jnp.float32, jnp.bfloat16
    rows, width = value_in.shape
    span = taps.shape[0]
    block = proj_weight.shape[1]
    planes = lax.axis_size("sp") // 4
    blocks = 2 * planes
    side = width // 2
    tiles = width // LANES
    step = max(n for n in (8, 16, 24, 32, 40) if rows % n == 0)
    kept = -(-(span + 2) // 8) * 8
    first, total = slot_table(planes, blocks)
    vmem, dma = pltpu.VMEM, pltpu.SemaphoreType.DMA
    scratch = [
        vmem((rows, width), bf16),
        vmem((rows, width), bf16),
        vmem((4, blocks, rows, block), bf16),
        vmem((blocks, side, block), bf16),
        vmem((tiles, kept, LANES), f32),
        vmem((tiles, rows + 2 * EDGE, LANES), f32),
        vmem((2, tiles, EDGE, LANES), bf16),
        vmem((2, tiles, EDGE, LANES), bf16),
        vmem((tiles, rows, LANES), f32),
        vmem((tiles, rows, LANES), f32),
        vmem((4, rows, LANES), f32),
        vmem((4, rows, LANES), f32),
        vmem((4, rows, LANES), f32),
        vmem((5, rows, side), bf16),
        vmem((tiles, rows, LANES), f32),
        vmem((tiles, rows, LANES), f32),
        vmem((4, rows, side), f32),
        vmem((2, rows, side), bf16),
        vmem((2, rows, side), bf16),
        vmem((rows, side), bf16),
        vmem((rows, side), bf16),
        vmem((blocks, side, block), f32),
        vmem((blocks, side, block), bf16),
        vmem((blocks, side, block), bf16),
        vmem((blocks, side, block), bf16),
        vmem((blocks, side, block), bf16),
        vmem((side, block), bf16),
        vmem((side, block), bf16),
        vmem((tiles, rows + 2 * EDGE, LANES), f32),
        vmem((2, tiles, EDGE, LANES), f32),
        vmem((2, tiles, EDGE, LANES), f32),
        vmem((tiles, kept, LANES), f32),
        vmem((3, tiles // 4, kept, LANES), f32),
        vmem((planes, tiles // 4, kept, LANES), f32),
        vmem((tiles // 4, kept, LANES), f32),
        vmem((tiles, kept, LANES), f32),
        vmem((rows, LANES), f32),
        dma((total,)),
        dma((total,)),
        dma((3 + blocks,)),
    ]
    whole, hbm = pl.BlockSpec(memory_space=pltpu.VMEM), pl.BlockSpec(memory_space=pl.ANY)
    outs = pl.pallas_call(
        functools.partial(kernel, (rows, width, span, planes, block, step), first),
        out_shape=(
            jax.ShapeDtypeStruct((rows, width), bf16),
            jax.ShapeDtypeStruct((rows, width), bf16),
            jax.ShapeDtypeStruct((span, width), f32),
            jax.ShapeDtypeStruct((1, width), f32),
            jax.ShapeDtypeStruct((1, width), f32),
            jax.ShapeDtypeStruct((width, block), f32),
        ),
        in_specs=[hbm, hbm, whole, whole, whole, hbm, hbm],
        out_specs=[whole] * 6,
        scratch_shapes=scratch,
        compiler_params=pltpu.CompilerParams(
            collective_id=0, has_side_effects=True, vmem_limit_bytes=62 * 2**20
        ),
    )(
        value_in,
        gate_in,
        taps,
        norm_gain.reshape(1, width),
        norm_bias.reshape(1, width),
        proj_weight,
        out_grad,
    )
    value_grad, gate_grad, tap_grad, gain_grad, bias_grad, weight_grad = outs
    return (
        value_grad,
        gate_grad,
        tap_grad,
        gain_grad.reshape(width),
        bias_grad.reshape(width),
        weight_grad,
    )


def solution(mesh):
    fused = mesh.shape["tp"] == 2 and mesh.shape["sp"] % 4 == 0
    return jax.shard_map(
        fused_on_device if fused else on_device,
        mesh=mesh,
        in_specs=(
            P("sp", "tp"),
            P("sp", "tp"),
            P(None, "tp"),
            P("tp"),
            P("tp"),
            P("tp", "sp"),
            P("sp", None),
        ),
        out_specs=(P("sp", "tp"), P("sp", "tp"), P(None, "tp"), P("tp"), P("tp"), P("tp", "sp")),
        check_vma=False,
    )
```

profile of v0, /device:TPU:0, one launch (start us, length us, event | category | flops | bytes accessed | tf_op | source)
XLA Modules:
  0.0 136.0 jit_solution(8253655358974173842)
XLA Ops:
  0.6 128.3 %shard_map.118 = (bf16[360,1024]{1,0:T(8,128)(2,1)}, bf16[360,1024]{1,0:T(8,128)(2,1)}, f32[31,1024]{1,0:T(8,128)}, f32[1,1024]{1,0:T(1,128)}, f32[1,1024]{1,0:T(1,128)}, /*index=5*/f32[1024,256]{1,0:T(8,128)}) custom-call(bf16[360,1024]{1,0:T(8,128)(2,1)} %value.1, bf16[360,1024]{1,0:T(8,128)(2,1)} %gate.1, f32[31,1024]{1,0:T(8,128)} %taps.1, ...), custom_call_target="tpu_custom_call" | custom-call | tf_op jit(solution)/shard_map/pallas_call | solution.py:834
  128.9 0.0 copy-start.1
  129.0 0.0 copy-start.3
  129.0 0.0 copy-start.2
  129.0 0.0 copy-start
  129.0 2.1 %copy.19 = bf16[360,1024]{1,0:T(8,128)(2,1)} copy(bf16[360,1024]{1,0:T(8,128)(2,1)} %get-tuple-element.24) | data formatting | bytes 1474560
  131.1 2.0 %copy.20 = bf16[360,1024]{1,0:T(8,128)(2,1)} copy(bf16[360,1024]{1,0:T(8,128)(2,1)} %get-tuple-element.25) | data formatting | bytes 1474560
  133.1 0.0 copy-done.1
  133.1 0.7 copy.21
  133.8 0.0 copy-done.3
  133.8 0.6 copy.22
  134.4 0.0 copy-done.2
  134.4 0.6 copy.23
  135.0 0.0 copy-done
  135.0 1.0 copy.24
Async XLA Ops:
  128.9 4.2 %copy-start.1 = (f32[31,1024]{1,0:T(8,128)S(1)}, f32[31,1024]{1,0:T(8,128)}, u32[]{:S(2)}) copy-start(f32[31,1024]{1,0:T(8,128)} %get-tuple-element.26) | copy-start | bytes 380932
  129.0 4.8 %copy-start.3 = (f32[1,1024]{1,0:T(1,128)S(1)}, f32[1,1024]{1,0:T(1,128)}, u32[]{:S(2)}) copy-start(f32[1,1024]{1,0:T(1,128)} %get-tuple-element.15) | copy-start | bytes 12292
  129.0 5.4 %copy-start.2 = (f32[1,1024]{1,0:T(1,128)S(1)}, f32[1,1024]{1,0:T(1,128)}, u32[]{:S(2)}) copy-start(f32[1,1024]{1,0:T(1,128)} %get-tuple-element.16) | copy-start | bytes 12292
  129.0 6.0 %copy-start = (f32[1024,256]{1,0:T(8,128)S(1)}, f32[1024,256]{1,0:T(8,128)}, u32[]{:S(2)}) copy-start(f32[1024,256]{1,0:T(8,128)} %get-tuple-element.29) | copy-start | bytes 3145732
where the time goes:
time: 138 us; the launch traced here: 136 us
  Pallas kernels  128 us (93%)
  local copies, waits for them, and re-layouts  6.97 us (5%)
    pallas_call x1, Pallas kernels, fused_on_device(): pl.pallas_call(functools.partial(kernel, (rows, width, span, planes, bloc...  128 us
    unnamed x14, local copies, waits for them, and re-layouts  6.97 us

commit v1 on v0

--- a/solution.py
+++ b/solution.py
@@ -169,8 +169,8 @@
         "act_x": 1,
         "act_y": 1,
         "act_d": 1,
-        "part_x": 2,
-        "part_y": 1,
+        "part_x": 4,
+        "part_y": 2,
         "up": blocks,
         "down": blocks,
         "w_back": 1,
@@ -231,6 +231,8 @@
     down_in,
     back_out,
     back_in,
+    weight_v,
+    turned,
     grads,
     gedge_out,
     gedge_in,
@@ -316,14 +318,21 @@
         return c * (blocks - 1) + q * (1 - 2 * c)
 
     mine = [index_of(core, q) for q in range(parts)]
-    other = [index_of(1 - core, q) for q in range(parts)]
+
+    def cols_at(slab, i):
+        return cols.at[slab, lax.div(i, 2), :, column(lax.rem(i, 2))]
+
+    def wh_at(zz, yy):
+        return wh.at[zz, :, column(yy)]
 
     load_v = pltpu.make_async_copy(value, value_v, local_sem.at[0])
     load_g = pltpu.make_async_copy(gate, gate_v, local_sem.at[1])
-    load_w = pltpu.make_async_copy(weight.at[my_rows], wh.at[z * 2 + y], local_sem.at[2])
+    load_w = pltpu.make_async_copy(weight.at[my_rows], wh_at(z, y), local_sem.at[2])
     load_c = [
         pltpu.make_async_copy(
-            cotangent.at[:, column(2 * i + x)], cols.at[0, i], local_sem.at[3 + i]
+            cotangent.at[:, column(2 * i + x)],
+            cols.at[0, i // 2, :, (i % 2) * block : (i % 2 + 1) * block],
+            local_sem.at[3 + i],
         )
         for i in range(blocks)
     ]
@@ -336,28 +345,27 @@
     peers += [(lax.rem(me + 1, count), core), (lax.rem(me + count - 1, count), core)]
     for peer in peers:
         pl.semaphore_signal(barrier, inc=1, device_id=peer, device_id_type=MESH)
-    pl.semaphore_wait(barrier, len(peers))
 
     def w_copies(d, p):
         yb = y if p == 0 else yn
         index = 2 * (d - 1) + p
-        below = wh.at[lax.rem(z - d + planes, planes) * 2 + yb]
-        above = wh.at[lax.rem(z + d, planes) * 2 + yb]
+        below = wh_at(lax.rem(z - d + planes, planes), yb)
+        above = wh_at(lax.rem(z + d, planes), yb)
         return (
             copy(below, below, "w_up", index, to_up),
             copy(above, above, "w_down", index, to_down),
         )
 
     def w_first(p, src, yb):
-        dst = wh.at[z * 2 + yb]
+        dst = wh_at(z, yb)
         send(copy(src, dst, "w_up", p, to_up), has_up)
         send(copy(src, dst, "w_down", p, to_down), has_down)
 
     def w_forward(d, p):
         up, down = w_copies(d, p)
         yb = y if p == 0 else yn
-        below = wh.at[lax.rem(z - d + planes, planes) * 2 + yb]
-        above = wh.at[lax.rem(z + d, planes) * 2 + yb]
+        below = wh_at(lax.rem(z - d + planes, planes), yb)
+        above = wh_at(lax.rem(z + d, planes), yb)
         arrive(up, z >= d)
         if d < planes - 1:
             send(copy(below, below, "w_up", 2 * d + p, to_up), jnp.logical_and(z >= d, has_up))
@@ -368,25 +376,23 @@
                 jnp.logical_and(z + d < planes, has_down),
             )
 
-    w_first(0, weight.at[my_rows], y)
-    w_y = copy(weight.at[their_rows], wh.at[z * 2 + y], "w_y", 0, to_y)
-    send(w_y)
+    w_y = copy(weight.at[their_rows], wh_at(z, y), "w_y", 0, to_y)
 
     def cols_x(q):
         return copy(
-            cotangent.at[:, column(2 * mine[q] + xn)], cols.at[1, mine[q]], "cols_x", q, to_x
+            cotangent.at[:, column(2 * mine[q] + xn)], cols_at(1, mine[q]), "cols_x", q, to_x
         )
 
     def cols_d(q):
-        return copy(cols.at[1, mine[q]], cols.at[3, mine[q]], "cols_d", q, to_y)
+        return copy(cols_at(1, mine[q]), cols_at(3, mine[q]), "cols_d", q, to_y)
 
     def cols_y(q):
         return copy(
-            cotangent.at[:, column(2 * mine[q] + x)], cols.at[2, mine[q]], "cols_y", q, to_y
+            cotangent.at[:, column(2 * mine[q] + x)], cols_at(2, mine[q]), "cols_y", q, to_y
         )
 
     def cols_core(slab, name, q):
-        ref = cols.at[slab, mine[q]]
+        ref = cols_at(slab, mine[q])
         return copy(ref, ref, name, q, to_core)
 
     def pass_x(q):
@@ -402,8 +408,6 @@
         arrive(cols_y(q))
         send(cols_core(2, "cols_y_core", q))
 
-    send(cols_x(0))
-
     def lay_taps(j):
         tap_t[j, 0:span, :] = taps[:, lanes(j)]
         small[j] = jnp.zeros(small.shape[1:], f32)
@@ -411,6 +415,9 @@
     over(tiles, lay_taps)
     load_v.wait()
     load_g.wait()
+    load_w.start()
+    for made in load_c:
+        made.start()
 
     def gate_tile(j):
         sig = jax.nn.sigmoid(gate_v[:, lanes(j)].astype(f32))
@@ -420,15 +427,16 @@
         edge_out[1, j] = mixed[j, EDGE : 2 * EDGE, :].astype(bf16)
 
     over(tiles, gate_tile)
+    pl.semaphore_wait(barrier, len(peers))
     halo_prev = copy(edge_out.at[0], edge_in.at[0], "halo", 0, to_next)
     halo_next = copy(edge_out.at[1], edge_in.at[1], "halo", 1, to_prev)
     send(halo_prev, has_next)
     send(halo_next, has_prev)
-    for q in range(1, parts):
+    w_first(0, weight.at[my_rows], y)
+    send(w_y)
+    send(cols_y(0))
+    for q in range(parts):
         send(cols_x(q))
-    load_w.start()
-    for made in load_c:
-        made.start()
 
     def fill(made, when, src, dst, at_row):
         @pl.when(when)
@@ -455,10 +463,6 @@
 
     over(tiles, conv_tile)
     pass_x(0)
-    arrive(w_y)
-    w_first(1, wh.at[z * 2 + yn], yn)
-    w_forward(1, 0)
-
     for r in range(0, rows, step):
         at_rows = slice(r, r + step)
         total = conv[0, at_rows, :]
@@ -474,7 +478,9 @@
         stat_out[1, at_rows, :] = square
     stats = copy(stat_out.at[0:2], stat_in.at[0:2], "stats", 0, to_core)
     send(stats)
-    pass_x(1) if parts > 1 else None
+    arrive(w_y)
+    w_first(1, wh_at(z, yn), yn)
+    w_forward(1, 0)
     arrive(stats)
     for r in range(0, rows, step):
         at_rows = slice(r, r + step)
@@ -506,13 +512,13 @@
     send(act_y)
     act_side(y)
     send(act_x)
-    w_forward(1, 1)
+    for q in range(1, parts):
+        pass_x(q)
+        if q == 1:
+            send(cols_y(1))
+            w_forward(1, 1)
     for q in range(2, parts):
-        pass_x(q)
-    for q in range(parts):
         send(cols_y(q))
-    if planes > 2:
-        w_forward(2, 0)
 
     def factor_tile(j):
         sig = jax.nn.sigmoid(gate_v[:, lanes(j)].astype(f32))
@@ -520,104 +526,152 @@
         factor_g[j] = value_v[:, lanes(j)].astype(f32) * sig * (1.0 - sig)
 
     over(tiles, factor_tile)
+    turned[0] = acts[y].T
+    if planes > 2:
+        w_forward(2, 0)
+    arrive(act_y)
+    send(act_d)
+    pass_d(0)
+    pass_y(0)
     if planes > 2:
         w_forward(2, 1)
-    arrive(act_y)
-    send(act_d)
+    arrive(act_x)
+    turned[1] = acts[2].T
+    turned[2] = acts[3].T
+    pass_d(1)
+    pass_y(1)
+    load_w.wait()
+    for made in load_c:
+        made.wait()
+
+    def weight_of(zb):
+        acc = jnp.dot(turned[0], cols[0, zb], preferred_element_type=f32)
+        for slab in range(1, 4):
+            acc = acc + jnp.dot(turned[slab], cols[slab, zb], preferred_element_type=f32)
+        wg[2 * zb] = acc[:, 0:block]
+        wg[2 * zb + 1] = acc[:, block : 2 * block]
+
+    def up_copy(t, p):
+        i = 2 * t + (yn if p == 0 else y)
+        return copy(up_out.at[i], up_in.at[i], "up", 2 * t + p, to_up)
+
+    def down_copy(t, p):
+        i = 2 * t + (yn if p == 0 else y)
+        return copy(down_out.at[i], down_in.at[i], "down", 2 * t + p, to_down)
+
+    def fresh(m):
+        for p in range(2):
+            for t, made, out, when in (
+                (planes - 1 - m, up_copy(planes - 1 - m, p), up_out, z == 0),
+                (m, down_copy(m, p), down_out, z == planes - 1),
+            ):
+                i = 2 * t + (yn if p == 0 else y)
+
+                @pl.when(when)
+                def _():
+                    out[i] = wg[i].astype(bf16)
+
+                send(made, when)
+
+    inner = jnp.logical_and(has_up, has_down)
+    lower = jnp.logical_and(inner, 2 * z < planes)
+    upper = jnp.logical_and(inner, 2 * z >= planes)
+
+    def relay(n, going_up, side_of):
+        m, p = n // 2, n % 2
+        t = planes - 1 - m if going_up else m
+        if not 0 <= m < planes - 1:
+            return
+        i = 2 * t + (yn if p == 0 else y)
+        made = up_copy(t, p) if going_up else down_copy(t, p)
+        out, got = (up_out, up_in) if going_up else (down_out, down_in)
+        when = jnp.logical_and(side_of, z < t if going_up else z > t)
+
+        @pl.when(when)
+        def _():
+            made.wait_recv()
+            out[i] = (wg[i] + got[i].astype(f32)).astype(bf16)
+
+        send(made, when)
+
+    def serve(n):
+        relay(n, True, lower)
+        relay(n - 1, False, lower)
+        relay(n, False, upper)
+        relay(n - 1, True, upper)
+
+    arrive(cols_core(3, "cols_d_core", 0))
+    arrive(cols_core(3, "cols_d_core", 1))
+    arrive(cols_core(1, "cols_x_core", 0))
+    arrive(cols_core(1, "cols_x_core", 1))
+    arrive(cols_core(2, "cols_y_core", 0))
+    arrive(cols_core(2, "cols_y_core", 1))
+    arrive(act_d)
+    turned[3] = acts[4].T
+    early = parts // 4
+    for zb in range(early):
+        weight_of(zb)
+        weight_of(planes - 1 - zb)
+        fresh(zb)
     for d in range(3, planes):
         w_forward(d, 0)
-    for q in range(parts):
+    for q in range(2, parts):
         pass_d(q)
     for d in range(3, planes):
         w_forward(d, 1)
-    load_w.wait()
-    for made in load_c:
-        made.wait()
 
     def product(slab):
-        def one(i):
+        acc = None
+        for zb in range(planes):
             got = lax.dot_general(
-                cols[slab, i], wh[i], (((1,), (1,)), ((), ())), preferred_element_type=f32
+                cols[slab, zb], wh[zb], (((1,), (1,)), ((), ())), preferred_element_type=f32
             )
-            part[slab] = part[slab] + got
-
-        part[slab] = lax.dot_general(
-            cols[slab, 0], wh[0], (((1,), (1,)), ((), ())), preferred_element_type=f32
-        )
-        lax.fori_loop(1, blocks, lambda i, c: (one(i), c)[1], 0)
-
-    part_x = [copy(part_out.at[n], part_in.at[n], "part_x", n, to_x) for n in range(2)]
+            acc = got if acc is None else acc + got
+        return acc
+
+    part_x = [
+        [copy(part_out.at[n, h], part_in.at[n, h], "part_x", 2 * n + h, to_x) for h in range(2)]
+        for n in range(2)
+    ]
+    cut = side // 2
 
     def partial(slab, n):
-        product(slab)
-        part_out[n] = part[slab].astype(bf16)
-        send(part_x[n])
-
-    for q in range(parts):
+        got = product(slab)
+        for h in range(2):
+            part_out[n, h] = got[:, h * cut : (h + 1) * cut].astype(bf16)
+            send(part_x[n][h])
+
+    for q in range(2, parts):
         arrive(cols_core(3, "cols_d_core", q))
     partial(3, 1)
-    for q in range(parts):
+    for q in range(2, parts):
         arrive(cols_core(1, "cols_x_core", q))
     partial(1, 0)
-
-    arrive(act_x)
-    arrive(act_d)
-
-    def weight_of(i):
-        acc = None
-        for slab, where in enumerate((y, 2, 3, 4)):
-            got = lax.dot_general(
-                acts[where],
-                cols[slab, i],
-                (((0,), (0,)), ((), ())),
-                preferred_element_type=f32,
-            )
-            acc = got if acc is None else acc + got
-        wg[i] = acc
-
-    for q in range(parts):
+    part[0] = product(0)
+    for q in range(2, parts):
         pass_y(q)
-        weight_of(mine[q])
+        if q == 2:
+            serve(0)
+    for q in range(2, parts):
         arrive(cols_core(2, "cols_y_core", q))
-        weight_of(other[q])
-
-    def up_copy(t, p):
-        i = 2 * t + (yn if p == 0 else y)
-        return copy(up_out.at[i], up_in.at[i], "up", 2 * t + p, to_up)
-
-    def down_copy(t, p):
-        i = 2 * t + (yn if p == 0 else y)
-        return copy(down_out.at[i], down_in.at[i], "down", 2 * t + p, to_down)
-
-    def relay(t, p, made, out, got, going, fresh):
-        i = 2 * t + (yn if p == 0 else y)
-
-        @pl.when(jnp.logical_and(going, fresh))
-        def _():
-            out[i] = wg[i].astype(bf16)
-
-        @pl.when(jnp.logical_and(going, jnp.logical_not(fresh)))
-        def _():
-            made.wait_recv()
-            out[i] = (wg[i] + got[i].astype(f32)).astype(bf16)
-
-        send(made, going)
-
-    def serve(m, p):
-        t = planes - 1 - m
-        relay(t, p, up_copy(t, p), up_out, up_in, z < t, z == 0)
-        relay(m, p, down_copy(m, p), down_out, down_in, z > m, z == planes - 1)
-
-    product(2)
-    serve(0, 0)
-    arrive(part_x[1])
-    half_out[...] = (part[2] + part_in[1].astype(f32)).astype(bf16)
-    part_y = copy(half_out, half_in, "part_y", 0, to_y)
-    send(part_y)
-    product(0)
-    serve(0, 1)
-    arrive(part_x[0])
-
+    part[1] = product(2)
+    part_y = [copy(half_out.at[h], half_in.at[h], "part_y", h, to_y) for h in range(2)]
+
+    def fold(h):
+        arrive(part_x[1][h])
+        got = part[1, :, h * cut : (h + 1) * cut] + part_in[1, h].astype(f32)
+        half_out[h] = got.astype(bf16)
+        send(part_y[h])
+
+    fold(0)
+    for zb in range(early, planes // 2):
+        weight_of(planes - 1 - zb)
+        weight_of(zb)
+        fresh(zb)
+    for m in range(planes // 2, planes - 1):
+        fresh(m)
+    fold(1)
+    serve(1)
     stat_out[2] = jnp.zeros((rows, LANES), f32)
     stat_out[3] = jnp.zeros((rows, LANES), f32)
 
@@ -632,20 +686,32 @@
         small[j, span : span + 1, :] = jnp.sum(crossed, axis=0, keepdims=True)
         small[j, span + 1 : span + 2, :] = jnp.sum(pre_grad, axis=0, keepdims=True)
 
-    def back_mine(jj):
-        got = part[0, :, lanes(jj)] + part_in[0, :, lanes(jj)].astype(f32)
-        back_tile(y * tiles_side + jj, got)
-
-    def back_theirs(jj):
-        back_tile(yn * tiles_side + jj, half_in[:, lanes(jj)].astype(f32))
-
-    over(tiles_side, back_mine)
-    arrive(part_y)
-    over(tiles_side, back_theirs)
+    tiles_cut = tiles_side // 2
+
+    def back_mine(h):
+        arrive(part_x[0][h])
+
+        def one(jj):
+            at_side = lanes(h * tiles_cut + jj)
+            got = part[0, :, at_side] + part_in[0, h, :, lanes(jj)].astype(f32)
+            back_tile(y * tiles_side + h * tiles_cut + jj, got)
+
+        over(tiles_cut, one)
+
+    def back_theirs(h):
+        arrive(part_y[h])
+
+        def one(jj):
+            back_tile(yn * tiles_side + h * tiles_cut + jj, half_in[h, :, lanes(jj)].astype(f32))
+
+        over(tiles_cut, one)
+
+    back_mine(0)
+    back_theirs(0)
+    back_mine(1)
+    back_theirs(1)
     norm = copy(stat_out.at[2:4], stat_in.at[2:4], "norm", 0, to_core)
     send(norm)
-    if planes > 2:
-        serve(1, 0)
     arrive(norm)
     for r in range(0, rows, step):
         at_rows = slice(r, r + step)
@@ -666,6 +732,7 @@
     grad_next = copy(gedge_out.at[1], gedge_in.at[1], "grad_halo", 1, to_prev)
     send(grad_prev, has_next)
     send(grad_next, has_prev)
+    serve(2)
 
     def tap_tile(j):
         def block_of(r, acc):
@@ -683,7 +750,6 @@
             small[j, k : k + 1, :] = jnp.sum(acc[k], axis=0, keepdims=True)
 
     over(tiles, tap_tile)
-
     place = 2 * y + x
     near = [(to_x, 2 * y + xn), (to_y, 2 * yn + x), (to_d, 2 * yn + xn)]
     own_tiles = pl.ds(place * quarter, quarter)
@@ -693,8 +759,6 @@
     ]
     for made in gather:
         send(made)
-    if planes > 2:
-        serve(1, 1)
     fill(grad_prev, has_prev, gedge_in.at[0], grads, 0)
     fill(grad_next, has_next, gedge_in.at[1], grads, EDGE + rows)
 
@@ -707,8 +771,8 @@
                 acc = acc + tap_t[j, k : k + 1, :] * grads[j, at_row : at_row + step, :]
             tile[r : r + step, :] = acc
         got = tile[...]
-        value_grad[:, lanes(j)] = (got * factor_v[j]).astype(bf16)
-        gate_grad[:, lanes(j)] = (got * factor_g[j]).astype(bf16)
+        value_v[:, lanes(j)] = (got * factor_v[j]).astype(bf16)
+        gate_v[:, lanes(j)] = (got * factor_g[j]).astype(bf16)
 
     def mixed_tiles(lo, hi):
         lax.fori_loop(lo, hi, lambda j, c: (mixed_tile(j), c)[1], 0)
@@ -720,23 +784,13 @@
     for d in range(1, planes):
         made = copy(across.at[z], across.at[z], "across", d, at(lax.rem(z + d, planes), y, x))
         send(made)
-    for m in range(2, planes - 1):
-        serve(m, 0)
+    for n in range(3, 2 * planes - 1):
+        serve(n)
     mixed_tiles(tiles_side, tiles)
-    for d in range(1, planes):
-        arrive(copy(across.at[z], across.at[z], "across", d, to_core))
-    total = across[0]
-    for d in range(1, planes):
-        total = total + across[d]
-    owned[...] = total
-    small_all[own_tiles] = total
-    spread_out = [
-        copy(owned, small_all.at[own_tiles], "plane_out", n, dev) for n, (dev, p) in enumerate(near)
-    ]
-    for made in spread_out:
-        send(made)
-    for m in range(2, planes - 1):
-        serve(m, 1)
+    store_v = pltpu.make_async_copy(value_v, value_grad, local_sem.at[0])
+    store_g = pltpu.make_async_copy(gate_v, gate_grad, local_sem.at[1])
+    store_v.start()
+    store_g.start()
 
     def finish(p):
         i = 2 * z + (yn if p == 0 else y)
@@ -754,25 +808,47 @@
                 if p == 0:
                     back_out[...] = total.astype(bf16)
                 else:
-                    weight_grad[my_rows, :] = total
-
+                    weight_v[0] = total
+
+    def across_out():
+        for d in range(1, planes):
+            arrive(copy(across.at[z], across.at[z], "across", d, to_core))
+        total = across[0]
+        for d in range(1, planes):
+            total = total + across[d]
+        owned[...] = total
+        small_all[own_tiles] = total
+        for made in spread_out:
+            send(made)
+
+    spread_out = [
+        copy(owned, small_all.at[own_tiles], "plane_out", n, dev) for n, (dev, p) in enumerate(near)
+    ]
     finish(0)
     back = copy(back_out, back_in, "w_back", 0, to_y)
     send(back)
+    across_out()
+    finish(1)
+    store_w = pltpu.make_async_copy(weight_v.at[0], weight_grad.at[my_rows], local_sem.at[2])
+    store_w.start()
     for made in spread_out:
         arrive(made)
     for j in range(tiles):
-        tap_grad[:, j * LANES : (j + 1) * LANES] = small_all[j, 0:span, :]
-        gain_grad[:, j * LANES : (j + 1) * LANES] = small_all[j, span : span + 1, :]
-        bias_grad[:, j * LANES : (j + 1) * LANES] = small_all[j, span + 1 : span + 2, :]
-    finish(1)
+        at_lanes = slice(j * LANES, (j + 1) * LANES)
+        tap_grad[:, at_lanes] = small_all[j, 0:span, :]
+        gain_grad[:, at_lanes] = small_all[j, span : span + 1, :]
+        bias_grad[:, at_lanes] = small_all[j, span + 1 : span + 2, :]
     arrive(back)
-    weight_grad[their_rows, :] = back_in[...].astype(f32)
+    weight_v[1] = back_in[...].astype(f32)
+    store_t = pltpu.make_async_copy(weight_v.at[1], weight_grad.at[their_rows], local_sem.at[3])
+    store_t.start()
     for made, when in pending:
         if when is None:
             made.wait_send()
         else:
             pl.when(when)(made.wait_send)
+    for made in (store_v, store_g, store_w, store_t):
+        made.wait()
 
 
 def fused_on_device(value_in, gate_in, taps, norm_gain, norm_bias, proj_weight, out_grad):
@@ -791,8 +867,8 @@
     scratch = [
         vmem((rows, width), bf16),
         vmem((rows, width), bf16),
-        vmem((4, blocks, rows, block), bf16),
-        vmem((blocks, side, block), bf16),
+        vmem((4, planes, rows, 2 * block), bf16),
+        vmem((planes, side, 2 * block), bf16),
         vmem((tiles, kept, LANES), f32),
         vmem((tiles, rows + 2 * EDGE, LANES), f32),
         vmem((2, tiles, EDGE, LANES), bf16),
@@ -805,11 +881,11 @@
         vmem((5, rows, side), bf16),
         vmem((tiles, rows, LANES), f32),
         vmem((tiles, rows, LANES), f32),
-        vmem((4, rows, side), f32),
-        vmem((2, rows, side), bf16),
-        vmem((2, rows, side), bf16),
-        vmem((rows, side), bf16),
-        vmem((rows, side), bf16),
+        vmem((2, rows, side), f32),
+        vmem((2, 2, rows, side // 2), bf16),
+        vmem((2, 2, rows, side // 2), bf16),
+        vmem((2, rows, side // 2), bf16),
+        vmem((2, rows, side // 2), bf16),
         vmem((blocks, side, block), f32),
         vmem((blocks, side, block), bf16),
         vmem((blocks, side, block), bf16),
@@ -817,6 +893,8 @@
         vmem((blocks, side, block), bf16),
         vmem((side, block), bf16),
         vmem((side, block), bf16),
+        vmem((2, side, block), f32),
+        vmem((4, side, rows), bf16),
         vmem((tiles, rows + 2 * EDGE, LANES), f32),
         vmem((2, tiles, EDGE, LANES), f32),
         vmem((2, tiles, EDGE, LANES), f32),
@@ -842,7 +920,7 @@
             jax.ShapeDtypeStruct((width, block), f32),
         ),
         in_specs=[hbm, hbm, whole, whole, whole, hbm, hbm],
-        out_specs=[whole] * 6,
+        out_specs=[hbm, hbm, whole, whole, whole, hbm],
         scratch_shapes=scratch,
         compiler_params=pltpu.CompilerParams(
             collective_id=0, has_side_effects=True, vmem_limit_bytes=62 * 2**20

time: 138 us -> 106 us (0.77)
  Pallas kernels: 128 us -> 97.7 us
    pallas_call x1, Pallas kernels: 128 us -> 97.7 us  [fused_on_device(): pl.pallas_call(functools.partial(kernel, (rows, width, span, planes, bloc...]
where the time goes in v1:
time: 106 us; the launch traced here: 105 us
  Pallas kernels  97.7 us (92%)
  local copies, waits for them, and re-layouts  6.97 us (7%)
    pallas_call x1, Pallas kernels, fused_on_device(): pl.pallas_call(functools.partial(kernel, (rows, width, span, planes, bloc...  97.7 us
    unnamed x14, local copies, waits for them, and re-layouts  6.97 us

profile of v1, /device:TPU:0, one launch (start us, length us, event | category | flops | bytes accessed | tf_op | source)
XLA Modules:
  0.0 105.3 jit_solution(6081532349891954342)
XLA Ops:
  0.6 97.7 %shard_map.118 = (bf16[360,1024]{1,0:T(8,128)(2,1)}, bf16[360,1024]{1,0:T(8,128)(2,1)}, f32[31,1024]{1,0:T(8,128)}, f32[1,1024]{1,0:T(1,128)}, f32[1,1024]{1,0:T(1,128)}, /*index=5*/f32[1024,256]{1,0:T(8,128)}) custom-call(bf16[360,1024]{1,0:T(8,128)(2,1)} %value.1, bf16[360,1024]{1,0:T(8,128)(2,1)} %gate.1, f32[31,1024]{1,0:T(8,128)} %taps.1, ...), custom_call_target="tpu_custom_call" | custom-call | tf_op jit(solution)/shard_map/pallas_call | solution.py:912
  98.3 0.0 copy-start.1
  98.3 0.0 copy-start.3
  98.3 0.0 copy-start.2
  98.3 0.0 copy-start
  98.4 2.1 %copy.19 = bf16[360,1024]{1,0:T(8,128)(2,1)} copy(bf16[360,1024]{1,0:T(8,128)(2,1)} %get-tuple-element.24) | data formatting | bytes 1474560
  100.5 2.0 %copy.20 = bf16[360,1024]{1,0:T(8,128)(2,1)} copy(bf16[360,1024]{1,0:T(8,128)(2,1)} %get-tuple-element.25) | data formatting | bytes 1474560
  102.5 0.0 copy-done.1
  102.5 0.7 copy.21
  103.2 0.0 copy-done.3
  103.2 0.6 copy.22
  103.8 0.0 copy-done.2
  103.8 0.6 copy.23
  104.4 0.0 copy-done
  104.4 1.0 copy.24
Async XLA Ops:
  98.3 4.2 %copy-start.1 = (f32[31,1024]{1,0:T(8,128)S(1)}, f32[31,1024]{1,0:T(8,128)}, u32[]{:S(2)}) copy-start(f32[31,1024]{1,0:T(8,128)} %get-tuple-element.26) | copy-start | bytes 380932
  98.3 4.8 %copy-start.3 = (f32[1,1024]{1,0:T(1,128)S(1)}, f32[1,1024]{1,0:T(1,128)}, u32[]{:S(2)}) copy-start(f32[1,1024]{1,0:T(1,128)} %get-tuple-element.15) | copy-start | bytes 12292
  98.3 5.4 %copy-start.2 = (f32[1,1024]{1,0:T(1,128)S(1)}, f32[1,1024]{1,0:T(1,128)}, u32[]{:S(2)}) copy-start(f32[1,1024]{1,0:T(1,128)} %get-tuple-element.16) | copy-start | bytes 12292
  98.3 6.0 %copy-start = (f32[1024,256]{1,0:T(8,128)S(1)}, f32[1024,256]{1,0:T(8,128)}, u32[]{:S(2)}) copy-start(f32[1024,256]{1,0:T(8,128)} %get-tuple-element.29) | copy-start | bytes 3145732

commit v2 on v1

--- a/solution.py
+++ b/solution.py
@@ -149,13 +149,14 @@
 
 LANES = 128
 EDGE = 16
+GROUP = 16
 MESH = pl.DeviceIdType.MESH
 
 
 def slot_table(planes, blocks):
     parts = blocks // 2
     sizes = {
-        "halo": 2,
+        "halo": 4,
         "cols_x": parts,
         "cols_x_core": parts,
         "cols_d": parts,
@@ -192,24 +193,25 @@
     first,
     value,
     gate,
-    taps,
-    gain,
-    bias,
+    taps_hbm,
+    gain_hbm,
+    bias_hbm,
     weight,
     cotangent,
     value_grad,
     gate_grad,
-    tap_grad,
-    gain_grad,
-    bias_grad,
-    weight_grad,
+    small_grad,
+    weight_mine,
+    weight_back,
     value_v,
     gate_v,
+    taps,
+    gain,
+    bias,
     cols,
     wh,
     tap_t,
     mixed,
-    edge_out,
     edge_in,
     conv,
     dact,
@@ -314,10 +316,15 @@
     def column(b):
         return pl.ds(pl.multiple_of(b * block, block), block)
 
-    def index_of(c, q):
-        return c * (blocks - 1) + q * (1 - 2 * c)
-
-    mine = [index_of(core, q) for q in range(parts)]
+    low = 2 * z < planes
+    turn = []
+    for q in range(planes - 1):
+        down_to = planes - 1 - q
+        fall = down_to - jnp.where(down_to <= z, 1, 0)
+        rise = q + jnp.where(q >= z, 1, 0)
+        turn.append(jnp.where(low, fall, rise))
+    turn.append(z)
+    mine = [2 * zb + core for zb in turn]
 
     def cols_at(slab, i):
         return cols.at[slab, lax.div(i, 2), :, column(lax.rem(i, 2))]
@@ -336,8 +343,10 @@
         )
         for i in range(blocks)
     ]
-    load_v.start()
-    load_g.start()
+    load_s = [
+        pltpu.make_async_copy(src, dst, local_sem.at[3 + blocks + n])
+        for n, (src, dst) in enumerate(((taps_hbm, taps), (gain_hbm, gain), (bias_hbm, bias)))
+    ]
 
     barrier = pltpu.get_barrier_semaphore()
     peers = [to_x, to_y, to_d, to_core]
@@ -345,6 +354,10 @@
     peers += [(lax.rem(me + 1, count), core), (lax.rem(me + count - 1, count), core)]
     for peer in peers:
         pl.semaphore_signal(barrier, inc=1, device_id=peer, device_id_type=MESH)
+    load_v.start()
+    load_g.start()
+    for made in load_s:
+        made.start()
 
     def w_copies(d, p):
         yb = y if p == 0 else yn
@@ -408,35 +421,41 @@
         arrive(cols_y(q))
         send(cols_core(2, "cols_y_core", q))
 
-    def lay_taps(j):
-        tap_t[j, 0:span, :] = taps[:, lanes(j)]
-        small[j] = jnp.zeros(small.shape[1:], f32)
-
-    over(tiles, lay_taps)
-    load_v.wait()
-    load_g.wait()
-    load_w.start()
-    for made in load_c:
-        made.start()
-
-    def gate_tile(j):
-        sig = jax.nn.sigmoid(gate_v[:, lanes(j)].astype(f32))
-        got = (value_v[:, lanes(j)].astype(f32) * sig).astype(bf16).astype(f32)
-        mixed[j, EDGE : EDGE + rows, :] = got
-        edge_out[0, j] = mixed[j, rows : rows + EDGE, :].astype(bf16)
-        edge_out[1, j] = mixed[j, EDGE : 2 * EDGE, :].astype(bf16)
-
-    over(tiles, gate_tile)
     pl.semaphore_wait(barrier, len(peers))
-    halo_prev = copy(edge_out.at[0], edge_in.at[0], "halo", 0, to_next)
-    halo_next = copy(edge_out.at[1], edge_in.at[1], "halo", 1, to_prev)
-    send(halo_prev, has_next)
-    send(halo_next, has_prev)
+    halo = []
+    for n, (src, near_rows) in enumerate(
+        ((value, rows - EDGE), (gate, rows - EDGE), (value, 0), (gate, 0))
+    ):
+        made = copy(
+            src.at[near_rows : near_rows + EDGE],
+            edge_in.at[n],
+            "halo",
+            n,
+            to_next if n < 2 else to_prev,
+        )
+        send(made, has_next if n < 2 else has_prev)
+        halo.append(made)
     w_first(0, weight.at[my_rows], y)
     send(w_y)
     send(cols_y(0))
     for q in range(parts):
         send(cols_x(q))
+    load_w.start()
+    for made in load_c:
+        made.start()
+    for made in load_s:
+        made.wait()
+    load_v.wait()
+    load_g.wait()
+
+    def gate_tile(j):
+        tap_t[j, 0:span, :] = taps[:, lanes(j)]
+        small[j] = jnp.zeros(small.shape[1:], f32)
+        sig = jax.nn.sigmoid(gate_v[:, lanes(j)].astype(f32))
+        got = (value_v[:, lanes(j)].astype(f32) * sig).astype(bf16).astype(f32)
+        mixed[j, EDGE : EDGE + rows, :] = got
+
+    over(tiles, gate_tile)
 
     def fill(made, when, src, dst, at_row):
         @pl.when(when)
@@ -450,8 +469,24 @@
             for j in range(tiles):
                 dst[j, at_row : at_row + EDGE, :] = jnp.zeros((EDGE, LANES), f32)
 
-    fill(halo_prev, has_prev, edge_in.at[0], mixed, 0)
-    fill(halo_next, has_next, edge_in.at[1], mixed, EDGE + rows)
+    def fill_mixed(first_of, when, at_row):
+        @pl.when(when)
+        def _():
+            halo[first_of].wait_recv()
+            halo[first_of + 1].wait_recv()
+            for j in range(tiles):
+                at_lanes = slice(j * LANES, (j + 1) * LANES)
+                sig = jax.nn.sigmoid(edge_in[first_of + 1, :, at_lanes].astype(f32))
+                got = edge_in[first_of, :, at_lanes].astype(f32) * sig
+                mixed[j, at_row : at_row + EDGE, :] = got.astype(bf16).astype(f32)
+
+        @pl.when(jnp.logical_not(when))
+        def _():
+            for j in range(tiles):
+                mixed[j, at_row : at_row + EDGE, :] = jnp.zeros((EDGE, LANES), f32)
+
+    fill_mixed(0, has_prev, 0)
+    fill_mixed(2, has_next, EDGE + rows)
 
     def conv_tile(j):
         for r in range(0, rows, step):
@@ -462,7 +497,6 @@
             conv[j, r : r + step, :] = acc
 
     over(tiles, conv_tile)
-    pass_x(0)
     for r in range(0, rows, step):
         at_rows = slice(r, r + step)
         total = conv[0, at_rows, :]
@@ -512,12 +546,14 @@
     send(act_y)
     act_side(y)
     send(act_x)
+    pass_x(0)
+    pass_x(1)
+    pass_y(0)
+    for q in range(2, parts - 1):
+        pass_x(q)
+    w_forward(1, 1)
+    pass_x(parts - 1)
     for q in range(1, parts):
-        pass_x(q)
-        if q == 1:
-            send(cols_y(1))
-            w_forward(1, 1)
-    for q in range(2, parts):
         send(cols_y(q))
 
     def factor_tile(j):
@@ -527,19 +563,17 @@
 
     over(tiles, factor_tile)
     turned[0] = acts[y].T
+    arrive(act_y)
+    send(act_d)
     if planes > 2:
         w_forward(2, 0)
-    arrive(act_y)
-    send(act_d)
-    pass_d(0)
-    pass_y(0)
-    if planes > 2:
-        w_forward(2, 1)
     arrive(act_x)
     turned[1] = acts[2].T
     turned[2] = acts[3].T
+    pass_d(0)
+    if planes > 2:
+        w_forward(2, 1)
     pass_d(1)
-    pass_y(1)
     load_w.wait()
     for made in load_c:
         made.wait()
@@ -559,238 +593,18 @@
         i = 2 * t + (yn if p == 0 else y)
         return copy(down_out.at[i], down_in.at[i], "down", 2 * t + p, to_down)
 
-    def fresh(m):
-        for p in range(2):
-            for t, made, out, when in (
-                (planes - 1 - m, up_copy(planes - 1 - m, p), up_out, z == 0),
-                (m, down_copy(m, p), down_out, z == planes - 1),
-            ):
-                i = 2 * t + (yn if p == 0 else y)
-
-                @pl.when(when)
-                def _():
-                    out[i] = wg[i].astype(bf16)
-
-                send(made, when)
-
-    inner = jnp.logical_and(has_up, has_down)
-    lower = jnp.logical_and(inner, 2 * z < planes)
-    upper = jnp.logical_and(inner, 2 * z >= planes)
-
-    def relay(n, going_up, side_of):
-        m, p = n // 2, n % 2
-        t = planes - 1 - m if going_up else m
-        if not 0 <= m < planes - 1:
-            return
-        i = 2 * t + (yn if p == 0 else y)
-        made = up_copy(t, p) if going_up else down_copy(t, p)
-        out, got = (up_out, up_in) if going_up else (down_out, down_in)
-        when = jnp.logical_and(side_of, z < t if going_up else z > t)
-
-        @pl.when(when)
-        def _():
-            made.wait_recv()
-            out[i] = (wg[i] + got[i].astype(f32)).astype(bf16)
-
-        send(made, when)
-
-    def serve(n):
-        relay(n, True, lower)
-        relay(n - 1, False, lower)
-        relay(n, False, upper)
-        relay(n - 1, True, upper)
-
-    arrive(cols_core(3, "cols_d_core", 0))
-    arrive(cols_core(3, "cols_d_core", 1))
-    arrive(cols_core(1, "cols_x_core", 0))
-    arrive(cols_core(1, "cols_x_core", 1))
-    arrive(cols_core(2, "cols_y_core", 0))
-    arrive(cols_core(2, "cols_y_core", 1))
-    arrive(act_d)
-    turned[3] = acts[4].T
-    early = parts // 4
-    for zb in range(early):
-        weight_of(zb)
-        weight_of(planes - 1 - zb)
-        fresh(zb)
-    for d in range(3, planes):
-        w_forward(d, 0)
-    for q in range(2, parts):
-        pass_d(q)
-    for d in range(3, planes):
-        w_forward(d, 1)
-
-    def product(slab):
-        acc = None
-        for zb in range(planes):
-            got = lax.dot_general(
-                cols[slab, zb], wh[zb], (((1,), (1,)), ((), ())), preferred_element_type=f32
-            )
-            acc = got if acc is None else acc + got
-        return acc
-
-    part_x = [
-        [copy(part_out.at[n, h], part_in.at[n, h], "part_x", 2 * n + h, to_x) for h in range(2)]
-        for n in range(2)
-    ]
-    cut = side // 2
-
-    def partial(slab, n):
-        got = product(slab)
-        for h in range(2):
-            part_out[n, h] = got[:, h * cut : (h + 1) * cut].astype(bf16)
-            send(part_x[n][h])
-
-    for q in range(2, parts):
-        arrive(cols_core(3, "cols_d_core", q))
-    partial(3, 1)
-    for q in range(2, parts):
-        arrive(cols_core(1, "cols_x_core", q))
-    partial(1, 0)
-    part[0] = product(0)
-    for q in range(2, parts):
-        pass_y(q)
-        if q == 2:
-            serve(0)
-    for q in range(2, parts):
-        arrive(cols_core(2, "cols_y_core", q))
-    part[1] = product(2)
-    part_y = [copy(half_out.at[h], half_in.at[h], "part_y", h, to_y) for h in range(2)]
-
-    def fold(h):
-        arrive(part_x[1][h])
-        got = part[1, :, h * cut : (h + 1) * cut] + part_in[1, h].astype(f32)
-        half_out[h] = got.astype(bf16)
-        send(part_y[h])
-
-    fold(0)
-    for zb in range(early, planes // 2):
-        weight_of(planes - 1 - zb)
-        weight_of(zb)
-        fresh(zb)
-    for m in range(planes // 2, planes - 1):
-        fresh(m)
-    fold(1)
-    serve(1)
-    stat_out[2] = jnp.zeros((rows, LANES), f32)
-    stat_out[3] = jnp.zeros((rows, LANES), f32)
-
-    def back_tile(j, got):
-        pre_grad = got * dact[j]
-        normed = conv[j]
-        scaled = pre_grad * gain[0:1, lanes(j)]
-        crossed = pre_grad * normed
-        dact[j] = scaled
-        stat_out[2] = stat_out[2] + scaled
-        stat_out[3] = stat_out[3] + scaled * normed
-        small[j, span : span + 1, :] = jnp.sum(crossed, axis=0, keepdims=True)
-        small[j, span + 1 : span + 2, :] = jnp.sum(pre_grad, axis=0, keepdims=True)
-
-    tiles_cut = tiles_side // 2
-
-    def back_mine(h):
-        arrive(part_x[0][h])
-
-        def one(jj):
-            at_side = lanes(h * tiles_cut + jj)
-            got = part[0, :, at_side] + part_in[0, h, :, lanes(jj)].astype(f32)
-            back_tile(y * tiles_side + h * tiles_cut + jj, got)
-
-        over(tiles_cut, one)
-
-    def back_theirs(h):
-        arrive(part_y[h])
-
-        def one(jj):
-            back_tile(yn * tiles_side + h * tiles_cut + jj, half_in[h, :, lanes(jj)].astype(f32))
-
-        over(tiles_cut, one)
-
-    back_mine(0)
-    back_theirs(0)
-    back_mine(1)
-    back_theirs(1)
-    norm = copy(stat_out.at[2:4], stat_in.at[2:4], "norm", 0, to_core)
-    send(norm)
-    arrive(norm)
-    for r in range(0, rows, step):
-        at_rows = slice(r, r + step)
-        for n in range(2):
-            both = stat_out[2 + n, at_rows, :] + stat_in[2 + n, at_rows, :]
-            got = jnp.sum(both, axis=1, keepdims=True) / (2 * width)
-            rows_of[2 + n, at_rows, :] = jnp.broadcast_to(got, (step, LANES))
-
-    def grad_tile(j):
-        grads[j, EDGE : EDGE + rows, :] = rows_of[1] * (
-            dact[j] - rows_of[2] - conv[j] * rows_of[3]
-        )
-        gedge_out[0, j] = grads[j, rows : rows + EDGE, :]
-        gedge_out[1, j] = grads[j, EDGE : 2 * EDGE, :]
-
-    over(tiles, grad_tile)
-    grad_prev = copy(gedge_out.at[0], gedge_in.at[0], "grad_halo", 0, to_next)
-    grad_next = copy(gedge_out.at[1], gedge_in.at[1], "grad_halo", 1, to_prev)
-    send(grad_prev, has_next)
-    send(grad_next, has_prev)
-    serve(2)
-
-    def tap_tile(j):
-        def block_of(r, acc):
-            base = pl.multiple_of(r * step, 8)
-            own = grads[j, pl.ds(base + EDGE, step), :]
-            out = []
-            for k in range(span):
-                got = own * mixed[j, pl.ds(base + k + lead, step), :]
-                out.append(acc[k] + jnp.sum(got.reshape(step // 8, 8, LANES), axis=0))
-            return tuple(out)
-
-        start = tuple(jnp.zeros((8, LANES), f32) for _ in range(span))
-        acc = lax.fori_loop(0, rows // step, block_of, start)
-        for k in range(span):
-            small[j, k : k + 1, :] = jnp.sum(acc[k], axis=0, keepdims=True)
-
-    over(tiles, tap_tile)
-    place = 2 * y + x
-    near = [(to_x, 2 * y + xn), (to_y, 2 * yn + x), (to_d, 2 * yn + xn)]
-    own_tiles = pl.ds(place * quarter, quarter)
-    gather = [
-        copy(small.at[pl.ds(p * quarter, quarter)], plane_in.at[n], "plane_in", n, dev)
-        for n, (dev, p) in enumerate(near)
-    ]
-    for made in gather:
-        send(made)
-    fill(grad_prev, has_prev, gedge_in.at[0], grads, 0)
-    fill(grad_next, has_next, gedge_in.at[1], grads, EDGE + rows)
-
-    def mixed_tile(j):
-        for r in range(0, rows, step):
-            at_row = r + EDGE + half
-            acc = tap_t[j, 0:1, :] * grads[j, at_row : at_row + step, :]
-            for k in range(1, span):
-                at_row = r + EDGE + half - k
-                acc = acc + tap_t[j, k : k + 1, :] * grads[j, at_row : at_row + step, :]
-            tile[r : r + step, :] = acc
-        got = tile[...]
-        value_v[:, lanes(j)] = (got * factor_v[j]).astype(bf16)
-        gate_v[:, lanes(j)] = (got * factor_g[j]).astype(bf16)
-
-    def mixed_tiles(lo, hi):
-        lax.fori_loop(lo, hi, lambda j, c: (mixed_tile(j), c)[1], 0)
-
-    mixed_tiles(0, tiles_side)
-    for made in gather:
-        arrive(made)
-    across[z] = small[own_tiles] + plane_in[0] + plane_in[1] + plane_in[2]
-    for d in range(1, planes):
-        made = copy(across.at[z], across.at[z], "across", d, at(lax.rem(z + d, planes), y, x))
-        send(made)
-    for n in range(3, 2 * planes - 1):
-        serve(n)
-    mixed_tiles(tiles_side, tiles)
-    store_v = pltpu.make_async_copy(value_v, value_grad, local_sem.at[0])
-    store_g = pltpu.make_async_copy(gate_v, gate_grad, local_sem.at[1])
-    store_v.start()
-    store_g.start()
+    def fresh(m, p):
+        for t, made, out, when in (
+            (planes - 1 - m, up_copy(planes - 1 - m, p), up_out, z == 0),
+            (m, down_copy(m, p), down_out, z == planes - 1),
+        ):
+            i = 2 * t + (yn if p == 0 else y)
+
+            @pl.when(when)
+            def _():
+                out[i] = wg[i].astype(bf16)
+
+            send(made, when)
 
     def finish(p):
         i = 2 * z + (yn if p == 0 else y)
@@ -808,14 +622,222 @@
                 if p == 0:
                     back_out[...] = total.astype(bf16)
                 else:
-                    weight_v[0] = total
+                    weight_v[...] = total
+
+    back = copy(back_out, back_in, "w_back", 0, to_y)
+    inner = jnp.logical_and(has_up, has_down)
+    lower = jnp.logical_and(inner, 2 * z < planes)
+    upper = jnp.logical_and(inner, 2 * z >= planes)
+
+    def relay(n, going_up, side_of):
+        m, p = n // 2, n % 2
+        t = planes - 1 - m if going_up else m
+        if not 0 <= m < planes - 1:
+            return
+        i = 2 * t + (yn if p == 0 else y)
+        made = up_copy(t, p) if going_up else down_copy(t, p)
+        out, got = (up_out, up_in) if going_up else (down_out, down_in)
+        when = jnp.logical_and(side_of, z < t if going_up else z > t)
+
+        @pl.when(when)
+        def _():
+            made.wait_recv()
+            out[i] = (wg[i] + got[i].astype(f32)).astype(bf16)
+
+        send(made, when)
+
+    def serve_near(n):
+        relay(n, True, lower)
+        relay(n, False, upper)
+
+    def serve_far(n):
+        relay(n, False, lower)
+        relay(n, True, upper)
+
+    def weigh(q):
+        arrive(cols_core(1, "cols_x_core", q))
+        arrive(cols_core(3, "cols_d_core", q))
+        arrive(cols_core(2, "cols_y_core", q))
+        weight_of(turn[q])
+
+    arrive(act_d)
+    turned[3] = acts[4].T
+    weigh(0)
+    fresh(0, 0)
+    fresh(0, 1)
+    for d in range(3, planes):
+        w_forward(d, 0)
+    for q in range(2, parts):
+        pass_d(q)
+    for d in range(3, planes):
+        w_forward(d, 1)
+
+    def product(slab):
+        acc = None
+        for zb in range(planes):
+            got = lax.dot_general(
+                cols[slab, zb], wh[zb], (((1,), (1,)), ((), ())), preferred_element_type=f32
+            )
+            acc = got if acc is None else acc + got
+        return acc
+
+    part_x = [
+        [copy(part_out.at[n, h], part_in.at[n, h], "part_x", 2 * n + h, to_x) for h in range(2)]
+        for n in range(2)
+    ]
+    cut = side // 2
+
+    def partial(slab, n):
+        got = product(slab)
+        for h in range(2):
+            part_out[n, h] = got[:, h * cut : (h + 1) * cut].astype(bf16)
+            send(part_x[n][h])
+
+    for q in range(1, parts):
+        arrive(cols_core(3, "cols_d_core", q))
+    partial(3, 1)
+    for q in range(1, parts):
+        arrive(cols_core(1, "cols_x_core", q))
+    partial(1, 0)
+    pass_y(1)
+    part[0] = product(0)
+    arrive(cols_core(2, "cols_y_core", 1))
+    weight_of(turn[1])
+    fresh(1, 0)
+    serve_near(0)
+    for q in range(2, parts):
+        pass_y(q)
+    for q in range(2, parts):
+        arrive(cols_core(2, "cols_y_core", q))
+    part[1] = product(2)
+    part_y = [copy(half_out.at[h], half_in.at[h], "part_y", h, to_y) for h in range(2)]
+
+    def fold(h):
+        arrive(part_x[1][h])
+        got = part[1, :, h * cut : (h + 1) * cut] + part_in[1, h].astype(f32)
+        half_out[h] = got.astype(bf16)
+        send(part_y[h])
+
+    fold(0)
+    for q in range(2, planes - 1):
+        weight_of(turn[q])
+        fresh(q, 0)
+        fresh(q - 1, 1)
+    serve_near(1)
+    serve_far(0)
+    fold(1)
+    weight_of(turn[planes - 1])
+    stat_out[2] = jnp.zeros((rows, LANES), f32)
+    stat_out[3] = jnp.zeros((rows, LANES), f32)
+
+    def back_tile(j, got):
+        pre_grad = got * dact[j]
+        normed = conv[j]
+        scaled = pre_grad * gain[0:1, lanes(j)]
+        crossed = pre_grad * normed
+        dact[j] = scaled
+        stat_out[2] = stat_out[2] + scaled
+        stat_out[3] = stat_out[3] + scaled * normed
+        small[j, span : span + 1, :] = jnp.sum(crossed, axis=0, keepdims=True)
+        small[j, span + 1 : span + 2, :] = jnp.sum(pre_grad, axis=0, keepdims=True)
+
+    tiles_cut = tiles_side // 2
+
+    def back_mine(h):
+        arrive(part_x[0][h])
+
+        def one(jj):
+            at_side = lanes(h * tiles_cut + jj)
+            got = part[0, :, at_side] + part_in[0, h, :, lanes(jj)].astype(f32)
+            back_tile(y * tiles_side + h * tiles_cut + jj, got)
+
+        over(tiles_cut, one)
+
+    def back_theirs(h):
+        arrive(part_y[h])
+
+        def one(jj):
+            back_tile(yn * tiles_side + h * tiles_cut + jj, half_in[h, :, lanes(jj)].astype(f32))
+
+        over(tiles_cut, one)
+
+    back_mine(0)
+    serve_near(2)
+    back_theirs(0)
+    back_mine(1)
+    back_theirs(1)
+    norm = copy(stat_out.at[2:4], stat_in.at[2:4], "norm", 0, to_core)
+    send(norm)
+    serve_far(1)
+    arrive(norm)
+    for r in range(0, rows, step):
+        at_rows = slice(r, r + step)
+        for n in range(2):
+            both = stat_out[2 + n, at_rows, :] + stat_in[2 + n, at_rows, :]
+            got = jnp.sum(both, axis=1, keepdims=True) / (2 * width)
+            rows_of[2 + n, at_rows, :] = jnp.broadcast_to(got, (step, LANES))
+
+    def grad_tile(j):
+        grads[j, EDGE : EDGE + rows, :] = rows_of[1] * (
+            dact[j] - rows_of[2] - conv[j] * rows_of[3]
+        )
+        gedge_out[0, j] = grads[j, rows : rows + EDGE, :]
+        gedge_out[1, j] = grads[j, EDGE : 2 * EDGE, :]
+
+    over(tiles, grad_tile)
+    grad_prev = copy(gedge_out.at[0], gedge_in.at[0], "grad_halo", 0, to_next)
+    grad_next = copy(gedge_out.at[1], gedge_in.at[1], "grad_halo", 1, to_prev)
+    send(grad_prev, has_next)
+    send(grad_next, has_prev)
+
+    def tap_tile(j):
+        for at in range(0, span, GROUP):
+            ks = range(at, min(at + GROUP, span))
+            acc = {}
+            for r in range(0, rows, step):
+                own = grads[j, r + EDGE : r + EDGE + step, :]
+                for k in ks:
+                    got = own * mixed[j, r + k + lead : r + k + lead + step, :]
+                    folded = jnp.sum(got.reshape(step // 8, 8, LANES), axis=0)
+                    acc[k] = acc[k] + folded if k in acc else folded
+            for k in ks:
+                small[j, k : k + 1, :] = jnp.sum(acc[k], axis=0, keepdims=True)
+
+    place = 2 * y + x
+    near = [(to_d, 2 * yn + xn), (to_x, 2 * y + xn), (to_y, 2 * yn + x)]
+    own_tiles = pl.ds(place * quarter, quarter)
+    gather = [
+        copy(small.at[pl.ds(p * quarter, quarter)], plane_in.at[n], "plane_in", n, dev)
+        for n, (dev, p) in enumerate(near)
+    ]
+    for n, (dev, p) in enumerate(near):
+        over(quarter, lambda jj: tap_tile(p * quarter + jj))
+        send(gather[n])
+    over(quarter, lambda jj: tap_tile(place * quarter + jj))
+    finish(0)
+    send(back)
+
+    def mixed_tile(j):
+        for r in range(0, rows, step):
+            at_row = r + EDGE + half
+            acc = tap_t[j, 0:1, :] * grads[j, at_row : at_row + step, :]
+            for k in range(1, span):
+                at_row = r + EDGE + half - k
+                acc = acc + tap_t[j, k : k + 1, :] * grads[j, at_row : at_row + step, :]
+            tile[r : r + step, :] = acc
+        got = tile[...]
+        value_v[:, lanes(j)] = (got * factor_v[j]).astype(bf16)
+        gate_v[:, lanes(j)] = (got * factor_g[j]).astype(bf16)
+
+    def mixed_tiles(lo, hi):
+        lax.fori_loop(lo, hi, lambda j, c: (mixed_tile(j), c)[1], 0)
 
     def across_out():
         for d in range(1, planes):
             arrive(copy(across.at[z], across.at[z], "across", d, to_core))
-        total = across[0]
+        total = across[0].astype(f32)
         for d in range(1, planes):
-            total = total + across[d]
+            total = total + across[d].astype(f32)
         owned[...] = total
         small_all[own_tiles] = total
         for made in spread_out:
@@ -824,30 +846,117 @@
     spread_out = [
         copy(owned, small_all.at[own_tiles], "plane_out", n, dev) for n, (dev, p) in enumerate(near)
     ]
-    finish(0)
-    back = copy(back_out, back_in, "w_back", 0, to_y)
-    send(back)
+    for made in gather:
+        arrive(made)
+    joined = small[own_tiles] + plane_in[0] + plane_in[1] + plane_in[2]
+    across[z] = joined.astype(bf16)
+    for d in range(1, planes):
+        made = copy(across.at[z], across.at[z], "across", d, at(lax.rem(z + d, planes), y, x))
+        send(made)
+    for n in range(3, 2 * (planes - 1)):
+        serve_near(n)
+        serve_far(n - 1)
+    serve_far(2 * planes - 3)
+    for m in range(2, planes - 1):
+        fresh(m, 1)
+    fill(grad_prev, has_prev, gedge_in.at[0], grads, 0)
+    fill(grad_next, has_next, gedge_in.at[1], grads, EDGE + rows)
+    mixed_tiles(0, 3 * quarter)
     across_out()
+    mixed_tiles(3 * quarter, tiles)
+    stores = [
+        pltpu.make_async_copy(value_v, value_grad, local_sem.at[0]),
+        pltpu.make_async_copy(gate_v, gate_grad, local_sem.at[1]),
+        pltpu.make_async_copy(weight_v, weight_mine, local_sem.at[2]),
+        pltpu.make_async_copy(small_all, small_grad, local_sem.at[3]),
+        pltpu.make_async_copy(back_in, weight_back, local_sem.at[4]),
+    ]
+    stores[0].start()
+    stores[1].start()
+
     finish(1)
-    store_w = pltpu.make_async_copy(weight_v.at[0], weight_grad.at[my_rows], local_sem.at[2])
-    store_w.start()
+    stores[2].start()
     for made in spread_out:
         arrive(made)
-    for j in range(tiles):
-        at_lanes = slice(j * LANES, (j + 1) * LANES)
-        tap_grad[:, at_lanes] = small_all[j, 0:span, :]
-        gain_grad[:, at_lanes] = small_all[j, span : span + 1, :]
-        bias_grad[:, at_lanes] = small_all[j, span + 1 : span + 2, :]
+    stores[3].start()
     arrive(back)
-    weight_v[1] = back_in[...].astype(f32)
-    store_t = pltpu.make_async_copy(weight_v.at[1], weight_grad.at[their_rows], local_sem.at[3])
-    store_t.start()
+    stores[4].start()
     for made, when in pending:
         if when is None:
             made.wait_send()
         else:
             pl.when(when)(made.wait_send)
-    for made in (store_v, store_g, store_w, store_t):
+    for made in stores:
+        made.wait()
+
+
+def write_out(
+    span,
+    value_in,
+    gate_in,
+    small_in,
+    mine_in,
+    back_in,
+    value_out,
+    gate_out,
+    tap_out,
+    gain_out,
+    bias_out,
+    weight_out,
+    value_v,
+    gate_v,
+    small_v,
+    mine_v,
+    back_v,
+    tap_v,
+    gain_v,
+    bias_v,
+    wide_v,
+    in_sem,
+    out_sem,
+):
+    side = mine_v.shape[0]
+    tiles = small_v.shape[0]
+    y = lax.rem(lax.div(lax.axis_index("sp"), 2), 2)
+
+    def rows_at(h):
+        return pl.ds(pl.multiple_of(h * side, side), side)
+
+    pairs = (
+        (back_in, back_v),
+        (small_in, small_v),
+        (value_in, value_v),
+        (gate_in, gate_v),
+        (mine_in, mine_v),
+    )
+    loads = [pltpu.make_async_copy(a, b, in_sem.at[n]) for n, (a, b) in enumerate(pairs)]
+    pairs = (
+        (wide_v, weight_out.at[rows_at(1 - y)]),
+        (tap_v, tap_out),
+        (gain_v, gain_out),
+        (bias_v, bias_out),
+        (value_v, value_out),
+        (gate_v, gate_out),
+        (mine_v, weight_out.at[rows_at(y)]),
+    )
+    stores = [pltpu.make_async_copy(a, b, out_sem.at[n]) for n, (a, b) in enumerate(pairs)]
+    for made in loads:
+        made.start()
+    loads[0].wait()
+    wide_v[...] = back_v[...].astype(jnp.float32)
+    stores[0].start()
+    loads[1].wait()
+    for j in range(tiles):
+        at_lanes = slice(j * LANES, (j + 1) * LANES)
+        tap_v[:, at_lanes] = small_v[j, 0:span, :]
+        gain_v[:, at_lanes] = small_v[j, span : span + 1, :]
+        bias_v[:, at_lanes] = small_v[j, span + 1 : span + 2, :]
+    for n in (1, 2, 3):
+        stores[n].start()
+    for n in (2, 3, 4):
+        loads[n].wait()
+        stores[n + 2].start()
+    for made in stores:
         made.wait()
 
 
@@ -867,12 +976,14 @@
     scratch = [
         vmem((rows, width), bf16),
         vmem((rows, width), bf16),
+        vmem((span, width), f32),
+        vmem((1, width), f32),
+        vmem((1, width), f32),
         vmem((4, planes, rows, 2 * block), bf16),
         vmem((planes, side, 2 * block), bf16),
         vmem((tiles, kept, LANES), f32),
         vmem((tiles, rows + 2 * EDGE, LANES), f32),
-        vmem((2, tiles, EDGE, LANES), bf16),
-        vmem((2, tiles, EDGE, LANES), bf16),
+        vmem((4, EDGE, width), bf16),
         vmem((tiles, rows, LANES), f32),
         vmem((tiles, rows, LANES), f32),
         vmem((4, rows, LANES), f32),
@@ -893,34 +1004,34 @@
         vmem((blocks, side, block), bf16),
         vmem((side, block), bf16),
         vmem((side, block), bf16),
-        vmem((2, side, block), f32),
+        vmem((side, block), f32),
         vmem((4, side, rows), bf16),
         vmem((tiles, rows + 2 * EDGE, LANES), f32),
         vmem((2, tiles, EDGE, LANES), f32),
         vmem((2, tiles, EDGE, LANES), f32),
         vmem((tiles, kept, LANES), f32),
         vmem((3, tiles // 4, kept, LANES), f32),
-        vmem((planes, tiles // 4, kept, LANES), f32),
+        vmem((planes, tiles // 4, kept, LANES), bf16),
         vmem((tiles // 4, kept, LANES), f32),
         vmem((tiles, kept, LANES), f32),
         vmem((rows, LANES), f32),
         dma((total,)),
         dma((total,)),
-        dma((3 + blocks,)),
+        dma((6 + blocks,)),
     ]
-    whole, hbm = pl.BlockSpec(memory_space=pltpu.VMEM), pl.BlockSpec(memory_space=pl.ANY)
-    outs = pl.pallas_call(
+    hbm = pl.BlockSpec(memory_space=pl.ANY)
+    values = jax.ShapeDtypeStruct((rows, width), bf16)
+    given = pl.pallas_call(
         functools.partial(kernel, (rows, width, span, planes, block, step), first),
         out_shape=(
-            jax.ShapeDtypeStruct((rows, width), bf16),
-            jax.ShapeDtypeStruct((rows, width), bf16),
-            jax.ShapeDtypeStruct((span, width), f32),
-            jax.ShapeDtypeStruct((1, width), f32),
-            jax.ShapeDtypeStruct((1, width), f32),
-            jax.ShapeDtypeStruct((width, block), f32),
+            values,
+            values,
+            jax.ShapeDtypeStruct((tiles, kept, LANES), f32),
+            jax.ShapeDtypeStruct((side, block), f32),
+            jax.ShapeDtypeStruct((side, block), bf16),
         ),
-        in_specs=[hbm, hbm, whole, whole, whole, hbm, hbm],
-        out_specs=[hbm, hbm, whole, whole, whole, hbm],
+        in_specs=[hbm] * 7,
+        out_specs=[hbm] * 5,
         scratch_shapes=scratch,
         compiler_params=pltpu.CompilerParams(
             collective_id=0, has_side_effects=True, vmem_limit_bytes=62 * 2**20
@@ -934,7 +1045,33 @@
         proj_weight,
         out_grad,
     )
-    value_grad, gate_grad, tap_grad, gain_grad, bias_grad, weight_grad = outs
+    value_grad, gate_grad, tap_grad, gain_grad, bias_grad, weight_grad = pl.pallas_call(
+        functools.partial(write_out, span),
+        out_shape=(
+            values,
+            values,
+            jax.ShapeDtypeStruct((span, width), f32),
+            jax.ShapeDtypeStruct((1, width), f32),
+            jax.ShapeDtypeStruct((1, width), f32),
+            jax.ShapeDtypeStruct((width, block), f32),
+        ),
+        in_specs=[hbm] * 5,
+        out_specs=[hbm] * 6,
+        scratch_shapes=[
+            vmem((rows, width), bf16),
+            vmem((rows, width), bf16),
+            vmem((tiles, kept, LANES), f32),
+            vmem((side, block), f32),
+            vmem((side, block), bf16),
+            vmem((span, width), f32),
+            vmem((1, width), f32),
+            vmem((1, width), f32),
+            vmem((side, block), f32),
+            dma((5,)),
+            dma((7,)),
+        ],
+        compiler_params=pltpu.CompilerParams(vmem_limit_bytes=62 * 2**20),
+    )(*given)
     return (
         value_grad,
         gate_grad,

time: 106 us -> 88.3 us (0.83)
  Pallas kernels: 97.7 us -> 87.5 us
  local copies, waits for them, and re-layouts: 6.97 us -> 0 us
    pallas_call x1, Pallas kernels: 97.7 us -> 84.8 us  [fused_on_device(): pl.pallas_call(functools.partial(kernel, (rows, width, span, planes, bloc...]
    unnamed x14 -> x0, local copies, waits for them, and re-layouts: 6.97 us -> none
    pallas_call x0 -> x1, Pallas kernels: none -> 2.66 us  [fused_on_device(): pl.pallas_call(functools.partial(write_out, span), out_shape=(values, val...]
where the time goes in v2:
time: 88.3 us; the launch traced here: 88.2 us
  Pallas kernels  87.5 us (99%)
    pallas_call x1, Pallas kernels, fused_on_device(): pl.pallas_call(functools.partial(kernel, (rows, width, span, planes, bloc...  84.8 us
    pallas_call x1, Pallas kernels, fused_on_device(): pl.pallas_call(functools.partial(write_out, span), out_shape=(values, val...  2.66 us

profile of v2, /device:TPU:0, one launch (start us, length us, event | category | flops | bytes accessed | tf_op | source)
XLA Modules:
  0.0 88.2 jit_solution(6794888875694425415)
XLA Ops:
  0.6 84.8 %shard_map.118 = (bf16[360,1024]{1,0:T(8,128)(2,1)}, bf16[360,1024]{1,0:T(8,128)(2,1)}, f32[8,40,128]{2,1,0:T(8,128)}, f32[512,256]{1,0:T(8,128)}, bf16[512,256]{1,0:T(8,128)(2,1)}) custom-call(bf16[360,1024]{1,0:T(8,128)(2,1)} %value.1, bf16[360,1024]{1,0:T(8,128)(2,1)} %gate.1, f32[31,1024]{1,0:T(8,128)} %taps_hbm.1, f32[1,1024]{1,0:T(1,128)} %bitcast.4, ...), custom_call_target="tpu_custom_call" | custom-call | tf_op jit(solution)/shard_map/pallas_call | solution.py:1024
  85.5 2.7 %shard_map.119 = (bf16[360,1024]{1,0:T(8,128)(2,1)}, bf16[360,1024]{1,0:T(8,128)(2,1)}, f32[31,1024]{1,0:T(8,128)}, f32[1,1024]{1,0:T(1,128)}, f32[1,1024]{1,0:T(1,128)}, /*index=5*/f32[1024,256]{1,0:T(8,128)}) custom-call(bf16[360,1024]{1,0:T(8,128)(2,1)} %get-tuple-element.17.value_in, bf16[360,1024]{1,0:T(8,128)(2,1)} %get-tuple-element.18.gate_in, ...), custom_call_target="tpu_custom_call" | custom-call | tf_op jit(solution)/shard_map/pallas_call | solution.py:1048

commit v3 on v2

--- a/solution.py
+++ b/solution.py
@@ -244,6 +244,7 @@
     owned,
     small_all,
     tile,
+    narrow,
     send_sem,
     recv_sem,
     local_sem,
@@ -578,12 +579,14 @@
     for made in load_c:
         made.wait()
 
-    def weight_of(zb):
-        acc = jnp.dot(turned[0], cols[0, zb], preferred_element_type=f32)
-        for slab in range(1, 4):
-            acc = acc + jnp.dot(turned[slab], cols[slab, zb], preferred_element_type=f32)
-        wg[2 * zb] = acc[:, 0:block]
-        wg[2 * zb + 1] = acc[:, block : 2 * block]
+    def weight_of(zb, lo=0, hi=4):
+        acc = None
+        for slab in range(lo, hi):
+            got = jnp.dot(turned[slab], cols[slab, zb], preferred_element_type=f32)
+            acc = got if acc is None else acc + got
+        for n in range(2):
+            got = acc[:, n * block : (n + 1) * block]
+            wg[2 * zb + n] = got if lo == 0 else wg[2 * zb + n] + got
 
     def up_copy(t, p):
         i = 2 * t + (yn if p == 0 else y)
@@ -654,15 +657,13 @@
         relay(n, False, lower)
         relay(n, True, upper)
 
-    def weigh(q):
-        arrive(cols_core(1, "cols_x_core", q))
-        arrive(cols_core(3, "cols_d_core", q))
-        arrive(cols_core(2, "cols_y_core", q))
-        weight_of(turn[q])
-
+    arrive(cols_core(1, "cols_x_core", 0))
+    arrive(cols_core(3, "cols_d_core", 0))
+    arrive(cols_core(2, "cols_y_core", 0))
+    weight_of(turn[0], 0, 3)
     arrive(act_d)
     turned[3] = acts[4].T
-    weigh(0)
+    weight_of(turn[0], 3, 4)
     fresh(0, 0)
     fresh(0, 1)
     for d in range(3, planes):
@@ -672,9 +673,9 @@
     for d in range(3, planes):
         w_forward(d, 1)
 
-    def product(slab):
+    def product(slab, over_zb=range(planes)):
         acc = None
-        for zb in range(planes):
+        for zb in over_zb:
             got = lax.dot_general(
                 cols[slab, zb], wh[zb], (((1,), (1,)), ((), ())), preferred_element_type=f32
             )
@@ -706,10 +707,11 @@
     fresh(1, 0)
     serve_near(0)
     for q in range(2, parts):
+        if q == parts - 1:
+            part[1] = product(2, turn[0 : parts - 1])
         pass_y(q)
-    for q in range(2, parts):
         arrive(cols_core(2, "cols_y_core", q))
-    part[1] = product(2)
+    part[1] = part[1] + product(2, turn[parts - 1 :])
     part_y = [copy(half_out.at[h], half_in.at[h], "part_y", h, to_y) for h in range(2)]
 
     def fold(h):
@@ -807,11 +809,13 @@
     near = [(to_d, 2 * yn + xn), (to_x, 2 * y + xn), (to_y, 2 * yn + x)]
     own_tiles = pl.ds(place * quarter, quarter)
     gather = [
-        copy(small.at[pl.ds(p * quarter, quarter)], plane_in.at[n], "plane_in", n, dev)
+        copy(narrow.at[pl.ds(p * quarter, quarter)], plane_in.at[n], "plane_in", n, dev)
         for n, (dev, p) in enumerate(near)
     ]
     for n, (dev, p) in enumerate(near):
         over(quarter, lambda jj: tap_tile(p * quarter + jj))
+        theirs = pl.ds(p * quarter, quarter)
+        narrow[theirs] = small[theirs].astype(bf16)
         send(gather[n])
     over(quarter, lambda jj: tap_tile(place * quarter + jj))
     finish(0)
@@ -848,7 +852,9 @@
     ]
     for made in gather:
         arrive(made)
-    joined = small[own_tiles] + plane_in[0] + plane_in[1] + plane_in[2]
+    joined = small[own_tiles]
+    for n in range(3):
+        joined = joined + plane_in[n].astype(f32)
     across[z] = joined.astype(bf16)
     for d in range(1, planes):
         made = copy(across.at[z], across.at[z], "across", d, at(lax.rem(z + d, planes), y, x))
@@ -1010,11 +1016,12 @@
         vmem((2, tiles, EDGE, LANES), f32),
         vmem((2, tiles, EDGE, LANES), f32),
         vmem((tiles, kept, LANES), f32),
-        vmem((3, tiles // 4, kept, LANES), f32),
+        vmem((3, tiles // 4, kept, LANES), bf16),
         vmem((planes, tiles // 4, kept, LANES), bf16),
         vmem((tiles // 4, kept, LANES), f32),
         vmem((tiles, kept, LANES), f32),
         vmem((rows, LANES), f32),
+        vmem((tiles, kept, LANES), bf16),
         dma((total,)),
         dma((total,)),
         dma((6 + blocks,)),

time: 88.3 us -> 86.9 us (0.984)
  Pallas kernels: 87.5 us -> 86.1 us
    pallas_call x1, Pallas kernels: 84.8 us -> 83.4 us  [fused_on_device(): pl.pallas_call(functools.partial(kernel, (rows, width, span, planes, bloc...]
where the time goes in v3:
time: 86.9 us; the launch traced here: 86.7 us
  Pallas kernels  86.1 us (99%)
    pallas_call x1, Pallas kernels, fused_on_device(): pl.pallas_call(functools.partial(kernel, (rows, width, span, planes, bloc...  83.4 us
    pallas_call x1, Pallas kernels, fused_on_device(): pl.pallas_call(functools.partial(write_out, span), out_shape=(values, val...  2.66 us

profile of v3, /device:TPU:0, one launch (start us, length us, event | category | flops | bytes accessed | tf_op | source)
XLA Modules:
  0.0 86.7 jit_solution(12290612403766389999)
XLA Ops:
  0.6 83.4 %shard_map.118 = (bf16[360,1024]{1,0:T(8,128)(2,1)}, bf16[360,1024]{1,0:T(8,128)(2,1)}, f32[8,40,128]{2,1,0:T(8,128)}, f32[512,256]{1,0:T(8,128)}, bf16[512,256]{1,0:T(8,128)(2,1)}) custom-call(bf16[360,1024]{1,0:T(8,128)(2,1)} %value.1, bf16[360,1024]{1,0:T(8,128)(2,1)} %gate.1, f32[31,1024]{1,0:T(8,128)} %taps_hbm.1, f32[1,1024]{1,0:T(1,128)} %bitcast.4, ...), custom_call_target="tpu_custom_call" | custom-call | tf_op jit(solution)/shard_map/pallas_call | solution.py:1031
  84.0 2.7 %shard_map.119 = (bf16[360,1024]{1,0:T(8,128)(2,1)}, bf16[360,1024]{1,0:T(8,128)(2,1)}, f32[31,1024]{1,0:T(8,128)}, f32[1,1024]{1,0:T(1,128)}, f32[1,1024]{1,0:T(1,128)}, /*index=5*/f32[1024,256]{1,0:T(8,128)}) custom-call(bf16[360,1024]{1,0:T(8,128)(2,1)} %get-tuple-element.17.value_in, bf16[360,1024]{1,0:T(8,128)(2,1)} %get-tuple-element.18.gate_in, ...), custom_call_target="tpu_custom_call" | custom-call | tf_op jit(solution)/shard_map/pallas_call | solution.py:1055

commit v4 on v3

--- a/solution.py
+++ b/solution.py
@@ -149,14 +149,14 @@
 
 LANES = 128
 EDGE = 16
-GROUP = 16
+GROUP = 31
 MESH = pl.DeviceIdType.MESH
 
 
 def slot_table(planes, blocks):
     parts = blocks // 2
     sizes = {
-        "halo": 4,
+        "halo": 2,
         "cols_x": parts,
         "cols_x_core": parts,
         "cols_d": parts,
@@ -212,6 +212,7 @@
     wh,
     tap_t,
     mixed,
+    edge_out,
     edge_in,
     conv,
     dact,
@@ -423,27 +424,9 @@
         send(cols_core(2, "cols_y_core", q))
 
     pl.semaphore_wait(barrier, len(peers))
-    halo = []
-    for n, (src, near_rows) in enumerate(
-        ((value, rows - EDGE), (gate, rows - EDGE), (value, 0), (gate, 0))
-    ):
-        made = copy(
-            src.at[near_rows : near_rows + EDGE],
-            edge_in.at[n],
-            "halo",
-            n,
-            to_next if n < 2 else to_prev,
-        )
-        send(made, has_next if n < 2 else has_prev)
-        halo.append(made)
     w_first(0, weight.at[my_rows], y)
     send(w_y)
-    send(cols_y(0))
-    for q in range(parts):
-        send(cols_x(q))
-    load_w.start()
-    for made in load_c:
-        made.start()
+    send(cols_x(0))
     for made in load_s:
         made.wait()
     load_v.wait()
@@ -455,8 +438,22 @@
         sig = jax.nn.sigmoid(gate_v[:, lanes(j)].astype(f32))
         got = (value_v[:, lanes(j)].astype(f32) * sig).astype(bf16).astype(f32)
         mixed[j, EDGE : EDGE + rows, :] = got
+        edge_out[0, j] = mixed[j, rows : rows + EDGE, :].astype(bf16)
+        edge_out[1, j] = mixed[j, EDGE : 2 * EDGE, :].astype(bf16)
 
     over(tiles, gate_tile)
+    halo = [
+        copy(edge_out.at[0], edge_in.at[0], "halo", 0, to_next),
+        copy(edge_out.at[1], edge_in.at[1], "halo", 1, to_prev),
+    ]
+    send(halo[0], has_next)
+    send(halo[1], has_prev)
+    send(cols_y(0))
+    for q in range(1, parts):
+        send(cols_x(q))
+    load_w.start()
+    for made in load_c:
+        made.start()
 
     def fill(made, when, src, dst, at_row):
         @pl.when(when)
@@ -474,20 +471,17 @@
         @pl.when(when)
         def _():
             halo[first_of].wait_recv()
-            halo[first_of + 1].wait_recv()
             for j in range(tiles):
-                at_lanes = slice(j * LANES, (j + 1) * LANES)
-                sig = jax.nn.sigmoid(edge_in[first_of + 1, :, at_lanes].astype(f32))
-                got = edge_in[first_of, :, at_lanes].astype(f32) * sig
-                mixed[j, at_row : at_row + EDGE, :] = got.astype(bf16).astype(f32)
+                mixed[j, at_row : at_row + EDGE, :] = edge_in[first_of, j].astype(f32)
 
         @pl.when(jnp.logical_not(when))
         def _():
             for j in range(tiles):
                 mixed[j, at_row : at_row + EDGE, :] = jnp.zeros((EDGE, LANES), f32)
 
+    pass_x(0)
     fill_mixed(0, has_prev, 0)
-    fill_mixed(2, has_next, EDGE + rows)
+    fill_mixed(1, has_next, EDGE + rows)
 
     def conv_tile(j):
         for r in range(0, rows, step):
@@ -547,7 +541,6 @@
     send(act_y)
     act_side(y)
     send(act_x)
-    pass_x(0)
     pass_x(1)
     pass_y(0)
     for q in range(2, parts - 1):
@@ -609,9 +602,9 @@
 
             send(made, when)
 
-    def finish(p):
+    def finish(p, among=range(planes)):
         i = 2 * z + (yn if p == 0 else y)
-        for t in range(planes):
+        for t in among:
 
             @pl.when(z == t)
             def _():
@@ -767,6 +760,8 @@
     serve_near(2)
     back_theirs(0)
     back_mine(1)
+    finish(0, sorted({0, planes - 1}))
+    send(back, jnp.logical_not(inner))
     back_theirs(1)
     norm = copy(stat_out.at[2:4], stat_in.at[2:4], "norm", 0, to_core)
     send(norm)
@@ -783,8 +778,8 @@
         grads[j, EDGE : EDGE + rows, :] = rows_of[1] * (
             dact[j] - rows_of[2] - conv[j] * rows_of[3]
         )
-        gedge_out[0, j] = grads[j, rows : rows + EDGE, :]
-        gedge_out[1, j] = grads[j, EDGE : 2 * EDGE, :]
+        gedge_out[0, j] = grads[j, rows : rows + EDGE, :].astype(bf16)
+        gedge_out[1, j] = grads[j, EDGE : 2 * EDGE, :].astype(bf16)
 
     over(tiles, grad_tile)
     grad_prev = copy(gedge_out.at[0], gedge_in.at[0], "grad_halo", 0, to_next)
@@ -806,7 +801,7 @@
                 small[j, k : k + 1, :] = jnp.sum(acc[k], axis=0, keepdims=True)
 
     place = 2 * y + x
-    near = [(to_d, 2 * yn + xn), (to_x, 2 * y + xn), (to_y, 2 * yn + x)]
+    near = [(to_d, 2 * yn + xn), (to_y, 2 * yn + x), (to_x, 2 * y + xn)]
     own_tiles = pl.ds(place * quarter, quarter)
     gather = [
         copy(narrow.at[pl.ds(p * quarter, quarter)], plane_in.at[n], "plane_in", n, dev)
@@ -818,8 +813,8 @@
         narrow[theirs] = small[theirs].astype(bf16)
         send(gather[n])
     over(quarter, lambda jj: tap_tile(place * quarter + jj))
-    finish(0)
-    send(back)
+    finish(0, range(1, planes - 1))
+    send(back, inner)
 
     def mixed_tile(j):
         for r in range(0, rows, step):
@@ -989,7 +984,8 @@
         vmem((planes, side, 2 * block), bf16),
         vmem((tiles, kept, LANES), f32),
         vmem((tiles, rows + 2 * EDGE, LANES), f32),
-        vmem((4, EDGE, width), bf16),
+        vmem((2, tiles, EDGE, LANES), bf16),
+        vmem((2, tiles, EDGE, LANES), bf16),
         vmem((tiles, rows, LANES), f32),
         vmem((tiles, rows, LANES), f32),
         vmem((4, rows, LANES), f32),
@@ -1013,8 +1009,8 @@
         vmem((side, block), f32),
         vmem((4, side, rows), bf16),
         vmem((tiles, rows + 2 * EDGE, LANES), f32),
-        vmem((2, tiles, EDGE, LANES), f32),
-        vmem((2, tiles, EDGE, LANES), f32),
+        vmem((2, tiles, EDGE, LANES), bf16),
+        vmem((2, tiles, EDGE, LANES), bf16),
         vmem((tiles, kept, LANES), f32),
         vmem((3, tiles // 4, kept, LANES), bf16),
         vmem((planes, tiles // 4, kept, LANES), bf16),

time: 86.9 us -> 85.6 us (0.985)
  Pallas kernels: 86.1 us -> 84.8 us
    pallas_call x1, Pallas kernels: 83.4 us -> 82.1 us  [fused_on_device(): pl.pallas_call(functools.partial(kernel, (rows, width, span, planes, bloc...]
where the time goes in v4:
time: 85.6 us; the launch traced here: 85.4 us
  Pallas kernels  84.8 us (99%)
    pallas_call x1, Pallas kernels, fused_on_device(): pl.pallas_call(functools.partial(kernel, (rows, width, span, planes, bloc...  82.1 us
    pallas_call x1, Pallas kernels, fused_on_device(): pl.pallas_call(functools.partial(write_out, span), out_shape=(values, val...  2.66 us

profile of v4, /device:TPU:0, one launch (start us, length us, event | category | flops | bytes accessed | tf_op | source)
XLA Modules:
  0.0 85.4 jit_solution(9503453604810011898)
XLA Ops:
  0.6 82.1 %shard_map.118 = (bf16[360,1024]{1,0:T(8,128)(2,1)}, bf16[360,1024]{1,0:T(8,128)(2,1)}, f32[8,40,128]{2,1,0:T(8,128)}, f32[512,256]{1,0:T(8,128)}, bf16[512,256]{1,0:T(8,128)(2,1)}) custom-call(bf16[360,1024]{1,0:T(8,128)(2,1)} %value.1, bf16[360,1024]{1,0:T(8,128)(2,1)} %gate.1, f32[31,1024]{1,0:T(8,128)} %taps_hbm.1, f32[1,1024]{1,0:T(1,128)} %bitcast.4, ...), custom_call_target="tpu_custom_call" | custom-call | tf_op jit(solution)/shard_map/pallas_call | solution.py:1027
  82.8 2.7 %shard_map.119 = (bf16[360,1024]{1,0:T(8,128)(2,1)}, bf16[360,1024]{1,0:T(8,128)(2,1)}, f32[31,1024]{1,0:T(8,128)}, f32[1,1024]{1,0:T(1,128)}, f32[1,1024]{1,0:T(1,128)}, /*index=5*/f32[1024,256]{1,0:T(8,128)}) custom-call(bf16[360,1024]{1,0:T(8,128)(2,1)} %get-tuple-element.17.value_in, bf16[360,1024]{1,0:T(8,128)(2,1)} %get-tuple-element.18.gate_in, ...), custom_call_target="tpu_custom_call" | custom-call | tf_op jit(solution)/shard_map/pallas_call | solution.py:1051
